TPU v7x, 32 devices: a whole 2x2x4 slice. The times are simulated.
32 devices in a mesh: sp: 16 (over z, y, x), tp: 2 (over core).
Axes of the slice: x: 2, y: 2, z: 4, core: 2. Of those that a mesh axis runs over, the one named last changes fastest.
Arguments:
- residual: bfloat16 [2048, 2048], P('sp'), may hold values from -6 to 6
- query_first: bfloat16 [2048, 8, 128], P('sp', 'tp'), may hold values from -6.5 to 6.5
- key_first: bfloat16 [2048, 8, 128], P('sp', 'tp'), may hold values from -6.5 to 6.5
- value_first: bfloat16 [2048, 8, 128], P('sp', 'tp'), may hold values from -6 to 6
- query_second: bfloat16 [2048, 8, 64], P('sp', 'tp'), may hold values from -6.5 to 6.5
- key_second: bfloat16 [2048, 8, 64], P('sp', 'tp'), may hold values from -6.5 to 6.5
- value_second: bfloat16 [2048, 8, 64], P('sp', 'tp'), may hold values from -6 to 6
- balance_first: float32 [8], P('tp'), may hold values from 0.3 to 0.8
- balance_second: float32 [8], P('tp'), may hold values from 0.3 to 0.8
- head_gain_first: float32 [128], replicated, may hold values from 0.1 to 1.9
- head_gain_second: float32 [64], replicated, may hold values from 0.1 to 1.9
- out_first: bfloat16 [1024, 2048], P('tp'), may hold values from -0.15625 to 0.15625
- out_second: bfloat16 [512, 2048], P('tp'), may hold values from -0.15625 to 0.15625
- mlp_gain: float32 [2048], replicated, may hold values from 0.1 to 1.9
- up_weight: bfloat16 [2048, 8192], P('sp', 'tp'), may hold values from -0.125 to 0.125
- down_weight: bfloat16 [2048, 8192], P('sp', 'tp'), may hold values from -0.0625 to 0.0625
Outputs:
- layer_out: bfloat16 [2048, 2048], P('sp')
All inputs are finite; a program needn't handle non-finite values.
Results may differ from a plain program's by a relative error of at most 0.018.
Values may be sent and summed in bfloat16 or wider, within the bound.
A program may use at most 128 MiB of HBM per device.

v0:
```python
import functools
import math

import jax
import jax.numpy as jnp
from jax import lax
from jax.experimental import pallas as pl
from jax.experimental.pallas import tpu as pltpu
from jax.sharding import PartitionSpec as P

DK_A = 64
DK_B = 32


EPSILON = 1e-06
HEAD_SCALE = 0.8


def attend(queries, keys, values, balance, gain, device, head_size):
    tokens = queries.shape[0]
    heads = queries.shape[1]
    seq = keys.shape[0]
    depth = values.shape[2]
    block = math.gcd(512, seq)
    scale = head_size ** (-0.5)
    query_maps = queries.reshape(tokens, heads, 2, head_size)
    key_maps = keys.reshape(seq, heads, 2, head_size)
    first_row = device * tokens
    positions = first_row + jnp.arange(tokens, dtype=jnp.int32)
    needed = (first_row + tokens + block - 1) // block

    def block_scores(number):
        start = number * block
        key_block = lax.dynamic_slice_in_dim(key_maps, start, block, 0)
        scores = (
            jnp.einsum("qhmd,khmd->hmqk", query_maps, key_block, preferred_element_type=jnp.float32)
            * scale
        )
        columns = start + jnp.arange(block, dtype=jnp.int32)
        visible = columns[None, :] <= positions[:, None]
        return (jnp.where(visible, scores, -jnp.inf), start)

    def statistics(number, carry):
        highest, total = carry
        scores, start = block_scores(number)
        fresh = jnp.maximum(highest, jnp.max(scores, axis=-1, keepdims=True))
        total = total * jnp.exp(highest - fresh) + jnp.sum(
            jnp.exp(scores - fresh), axis=-1, keepdims=True
        )
        return (fresh, total)

    start_high = jnp.full((heads, 2, tokens, 1), -jnp.inf, jnp.float32)
    start_total = jnp.zeros((heads, 2, tokens, 1), jnp.float32)
    highest, total = lax.fori_loop(0, needed, statistics, (start_high, start_total))

    def accumulate(number, result):
        scores, start = block_scores(number)
        probs = jnp.exp(scores - highest) / total
        mixed = (probs[:, 0] - balance[:, None, None] * probs[:, 1]).astype(jnp.bfloat16)
        value_block = lax.dynamic_slice_in_dim(values, start, block, 0)
        return result + jnp.einsum(
            "hqk,khe->qhe", mixed, value_block, preferred_element_type=jnp.float32
        )

    summed = lax.fori_loop(0, needed, accumulate, jnp.zeros((tokens, heads, depth), jnp.float32))
    power = jnp.mean(summed * summed, axis=-1, keepdims=True)
    normed = summed * lax.rsqrt(power + EPSILON) * gain * HEAD_SCALE
    return normed.astype(jnp.bfloat16).reshape(tokens, heads * depth)


def body(
    residual,
    query_first,
    key_first,
    value_first,
    query_second,
    key_second,
    value_second,
    balance_first,
    balance_second,
    head_gain_first,
    head_gain_second,
    out_first,
    out_second,
    mlp_gain,
    up_weight,
    down_weight,
):
    device = lax.axis_index("sp")
    keys_first, values_first, keys_second, values_second = (
        lax.all_gather(key_first, "sp", axis=0, tiled=True),
        lax.all_gather(value_first, "sp", axis=0, tiled=True),
        lax.all_gather(key_second, "sp", axis=0, tiled=True),
        lax.all_gather(value_second, "sp", axis=0, tiled=True),
    )
    heads_first = attend(
        query_first, keys_first, values_first, balance_first, head_gain_first, device, DK_A
    )
    heads_second = attend(
        query_second, keys_second, values_second, balance_second, head_gain_second, device, DK_B
    )
    head_term = jnp.dot(heads_first, out_first, preferred_element_type=jnp.float32) + jnp.dot(
        heads_second, out_second, preferred_element_type=jnp.float32
    )
    head_total = lax.psum(head_term.astype(jnp.bfloat16), "tp").astype(jnp.float32)
    mixed = (residual.astype(jnp.float32) + head_total).astype(jnp.bfloat16)
    mixed_float = mixed.astype(jnp.float32)
    power = jnp.mean(mixed_float * mixed_float, axis=-1, keepdims=True)
    normed = (mixed_float * lax.rsqrt(power + EPSILON) * mlp_gain).astype(jnp.bfloat16)
    up_whole, down_whole = (
        lax.all_gather(up_weight, "sp", axis=0, tiled=True),
        lax.all_gather(down_weight, "sp", axis=0, tiled=True),
    )
    lifted = jnp.dot(normed, up_whole, preferred_element_type=jnp.float32)
    active = jax.nn.relu(lifted)
    hidden = (active * active).astype(jnp.bfloat16)
    down_term = lax.dot_general(
        hidden, down_whole, (((1,), (1,)), ((), ())), preferred_element_type=jnp.float32
    )
    added = lax.psum(down_term.astype(jnp.bfloat16), "tp").astype(jnp.float32)
    return (mixed_float + added).astype(jnp.bfloat16)


PLANE = 4
MESH = pl.DeviceIdType.MESH
VMEM_BYTES = 60 * 1024 * 1024


def remote(src, dst, send_sem, recv_sem, device):
    return pltpu.make_async_remote_copy(
        src_ref=src, dst_ref=dst, send_sem=send_sem, recv_sem=recv_sem,
        device_id=device, device_id_type=MESH,
    )


def meet(devices):
    barrier = pltpu.get_barrier_semaphore()
    for device in devices:
        pl.semaphore_signal(barrier, inc=1, device_id=device, device_id_type=MESH)
    pl.semaphore_wait(barrier, len(devices))


def places():
    s = lax.axis_index("sp")
    c = lax.axis_index("tp")
    z = s // PLANE
    p = s % PLANE
    x = p % 2
    y = p // 2
    flip_x = y * 2 + 1 - x
    flip_y = (1 - y) * 2 + x
    near = (1 - c) * flip_x + c * flip_y
    side = (1 - c) * flip_y + c * flip_x
    far = (1 - y) * 2 + 1 - x
    return s, c, z, p, near, side, far


def exchange_kernel(
    line, kv, q, up, down, kv_all, q_all, up_all, down_all,
    local, zs, zr, qs, qr, ps, pr, us, ur, ds, dr,
):
    s, c, z, p, near, side, far = places()
    n = line * PLANE
    width = up_all.shape[2]
    meet([((s + k) % n, c) for k in range(1, n)])
    own = pl.ds(pl.multiple_of(s * width, width), width)
    locals_ = [
        pltpu.make_async_copy(kv.at[z], kv_all.at[s], local.at[0]),
        pltpu.make_async_copy(q.at[z], q_all.at[z], local.at[1]),
        pltpu.make_async_copy(up.at[:, own], up_all.at[s], local.at[2]),
        pltpu.make_async_copy(down.at[:, own], down_all.at[s], local.at[3]),
    ]
    for copy in locals_:
        copy.start()
    sends = []

    def send(*args):
        copy = remote(*args)
        copy.start()
        sends.append(copy)

    for j in range(1, line):
        zt = (z + j) % line
        to = (zt * PLANE + p, c)
        send(kv.at[zt], kv_all.at[s], zs.at[j], zr.at[j], to)
        send(q.at[zt], q_all.at[z], qs.at[j], qr.at[j], to)

    def weights(ks):
        for k in ks:
            t = (s + k) % n
            columns = pl.ds(pl.multiple_of(t * width, width), width)
            send(up.at[:, columns], up_all.at[s], us.at[k], ur.at[k], (t, c))
            send(down.at[:, columns], down_all.at[s], ds.at[k], dr.at[k], (t, c))

    ring = list(range(1, n))
    share = -(-len(ring) // line)
    locals_[0].wait()
    to_near = (z * PLANE + near, c)
    to_side = (z * PLANE + side, c)
    for j in range(line):
        zf = (z + line - j) % line
        block = kv_all.at[zf * PLANE + p]
        if j:
            remote(block, block, zs.at[j], zr.at[j], to_near).wait_recv()
        send(block, block, ps.at[j, 0], pr.at[j, 0], to_near)
        send(block, block, ps.at[j, 1], pr.at[j, 1], to_side)
        weights(ring[j * share:(j + 1) * share])
    for j in range(line):
        zf = (z + line - j) % line
        block = kv_all.at[zf * PLANE + near]
        remote(block, block, ps.at[j, 0], pr.at[j, 0], to_near).wait_recv()
        send(block, block, ps.at[j, 2], pr.at[j, 2], to_side)
    for j in range(line):
        zf = (z + line - j) % line
        for way, place in ((1, side), (2, far)):
            block = kv_all.at[zf * PLANE + place]
            remote(block, block, ps.at[j, way], pr.at[j, way], to_side).wait_recv()
    for j in range(1, line):
        zf = (z + line - j) % line
        block = q_all.at[zf]
        remote(block, block, qs.at[j], qr.at[j], to_near).wait_recv()
    for k in range(1, n):
        f = (s + n - k) % n
        remote(up_all.at[f], up_all.at[f], us.at[k], ur.at[k], to_near).wait_recv()
        remote(down_all.at[f], down_all.at[f], ds.at[k], dr.at[k], to_near).wait_recv()
    for copy in locals_[1:]:
        copy.wait()
    for copy in sends:
        copy.wait_send()


def exchange(line, kv, q, up, down):
    n = line * PLANE
    width = up.shape[1] // n
    dma = pltpu.SemaphoreType.DMA
    vmem = pl.BlockSpec(memory_space=pltpu.VMEM)
    return pl.pallas_call(
        functools.partial(exchange_kernel, line),
        out_shape=(
            jax.ShapeDtypeStruct((n,) + kv.shape[1:], kv.dtype),
            jax.ShapeDtypeStruct(q.shape, q.dtype),
            jax.ShapeDtypeStruct((n, up.shape[0], width), up.dtype),
            jax.ShapeDtypeStruct((n, down.shape[0], width), down.dtype),
        ),
        in_specs=[vmem] * 4,
        out_specs=(vmem,) * 4,
        scratch_shapes=[
            dma((4,)), dma((line,)), dma((line,)), dma((line,)), dma((line,)),
            dma((line, 3)), dma((line, 3)), dma((n,)), dma((n,)), dma((n,)), dma((n,)),
        ],
        compiler_params=pltpu.CompilerParams(
            collective_id=0, has_side_effects=True, vmem_limit_bytes=32 * 1024 * 1024
        ),
    )(kv, q, up, down)


def last(a, b):
    return lax.dot_general(a, b, (((1,), (1,)), ((), ())), preferred_element_type=jnp.float32)


def attention_kernel(line, size_a, size_b, balance, q, kv, gain_a, gain_b, out):
    s, c, z, p, _, _, _ = places()
    tokens = q.shape[1]
    wide = gain_a.shape[1]
    deep = gain_b.shape[1]
    span = PLANE * tokens
    lanes = lax.broadcasted_iota(jnp.int32, (tokens, wide), 1)
    rows = lax.broadcasted_iota(jnp.int32, (tokens, span), 0) + p * tokens
    visible = lax.broadcasted_iota(jnp.int32, (tokens, span), 1) <= rows

    def mix(queries, keys_at, values_at, size, b, keys_number):
        maps = []
        for m in range(2):
            chosen = (lanes >= m * size) & (lanes < (m + 1) * size)
            picked = jnp.where(chosen, queries, jnp.zeros_like(queries))
            scores = last(picked, kv[0:keys_number, keys_at]) * size ** (-0.5)
            tail_scores = jnp.where(visible, scores[:, keys_number - span:], -jnp.inf)
            if keys_number > span:
                scores = jnp.concatenate([scores[:, : keys_number - span], tail_scores], axis=1)
            else:
                scores = tail_scores
            powers = jnp.exp(scores - jnp.max(scores, axis=-1, keepdims=True))
            maps.append((powers, jnp.sum(powers, axis=-1, keepdims=True)))
        (e1, l1), (e2, l2) = maps
        weights = (e1 * (1.0 / l1) - e2 * (b / l2)).astype(jnp.bfloat16)
        return jnp.dot(weights, kv[0:keys_number, values_at], preferred_element_type=jnp.float32)

    def norm(mixed, gain):
        power = jnp.mean(mixed * mixed, axis=-1, keepdims=True)
        return (mixed * lax.rsqrt(power + EPSILON) * gain[...] * HEAD_SCALE).astype(jnp.bfloat16)

    for j in range(line):
        number = (j + 1) * span
        first = mix(q[j, :, 0:wide], slice(0, wide), slice(wide, 2 * wide), size_a, balance[0], number)
        out[j, :, 0:wide] = norm(first, gain_a)
        both = slice(2 * wide, 3 * wide)
        second = mix(q[j, :, wide:2 * wide], both, both, size_b, balance[1], number)
        out[j, :, wide:wide + deep] = norm(second[:, wide - deep:wide], gain_b)


def attention(line, size_a, size_b, balance, q, kv, gain_a, gain_b):
    vmem = pl.BlockSpec(memory_space=pltpu.VMEM)
    shape = (line, q.shape[1], gain_a.shape[1] + gain_b.shape[1])
    return pl.pallas_call(
        functools.partial(attention_kernel, line, size_a, size_b),
        out_shape=jax.ShapeDtypeStruct(shape, jnp.bfloat16),
        in_specs=[pl.BlockSpec(memory_space=pltpu.SMEM)] + [vmem] * 4,
        out_specs=vmem,
        compiler_params=pltpu.CompilerParams(vmem_limit_bytes=32 * 1024 * 1024),
    )(balance, q, kv, gain_a, gain_b)


def return_kernel(line, heads, gathered, local, zs, zr):
    s, c, z, p, _, _, _ = places()
    meet([(((z + j) % line) * PLANE + p, c) for j in range(1, line)])
    mine = pltpu.make_async_copy(heads.at[z], gathered.at[z], local)
    mine.start()
    sends = []
    for j in range(1, line):
        zt = (z + j) % line
        copy = remote(heads.at[zt], gathered.at[z], zs.at[j], zr.at[j], (zt * PLANE + p, c))
        copy.start()
        sends.append(copy)
    for j in range(1, line):
        block = gathered.at[(z + line - j) % line]
        remote(block, block, zs.at[j], zr.at[j], (s, 1 - c)).wait_recv()
    mine.wait()
    for copy in sends:
        copy.wait_send()


def return_heads(line, heads):
    dma = pltpu.SemaphoreType.DMA
    vmem = pl.BlockSpec(memory_space=pltpu.VMEM)
    return pl.pallas_call(
        functools.partial(return_kernel, line),
        out_shape=jax.ShapeDtypeStruct(heads.shape, heads.dtype),
        in_specs=[vmem],
        out_specs=vmem,
        scratch_shapes=[dma, dma((line,)), dma((line,))],
        compiler_params=pltpu.CompilerParams(collective_id=1, has_side_effects=True),
    )(heads)


def gather_kernel(
    line, residual, part, gain, mixed, rows, other_part, xs, xr, zs, zr, ps, pr, cs, cr
):
    s, c, z, p, near, side, far = places()
    to_near = (z * PLANE + near, c)
    to_side = (z * PLANE + side, c)
    to_core = (s, 1 - c)
    meet(
        [to_near, to_side, to_core]
        + [(((z + j) % line) * PLANE + p, c) for j in range(1, line)]
    )
    swap = remote(part.at[1 - c], other_part, xs, xr, to_core)
    swap.start()
    swap.wait()
    total = part[c].astype(jnp.float32) + other_part[...].astype(jnp.float32)
    mixed[...] = (residual[c].astype(jnp.float32) + total).astype(jnp.bfloat16)
    whole = mixed[...].astype(jnp.float32)
    power = jnp.mean(whole * whole, axis=-1, keepdims=True)
    rows[s * 2 + c] = (whole * lax.rsqrt(power + EPSILON) * gain[...]).astype(jnp.bfloat16)
    sends = []

    def send(block, send_sem, recv_sem, device):
        copy = remote(block, block, send_sem, recv_sem, device)
        copy.start()
        sends.append(copy)

    def arrived(block, send_sem, recv_sem):
        remote(block, block, send_sem, recv_sem, to_core).wait_recv()

    def slot(j, place, core):
        return rows.at[(((z + line - j) % line) * PLANE + place) * 2 + core]

    for j in range(1, line):
        send(slot(0, p, c), zs.at[j], zr.at[j], (((z + j) % line) * PLANE + p, c))
    for j in range(line + 1):
        if j < line:
            block = slot(j, p, c)
            if j:
                arrived(block, zs.at[j], zr.at[j])
            send(block, ps.at[j, 0], pr.at[j, 0], to_near)
            send(block, ps.at[j, 1], pr.at[j, 1], to_side)
            send(block, cs.at[j, 0], cr.at[j, 0], to_core)
        if j:
            block = slot(j - 1, near, c)
            arrived(block, ps.at[j - 1, 0], pr.at[j - 1, 0])
            send(block, ps.at[j - 1, 2], pr.at[j - 1, 2], to_side)
            send(block, cs.at[j - 1, 1], cr.at[j - 1, 1], to_core)
    for j in range(line):
        for way, place in ((1, side), (2, far)):
            block = slot(j, place, c)
            arrived(block, ps.at[j, way], pr.at[j, way])
            send(block, cs.at[j, 1 + way], cr.at[j, 1 + way], to_core)
    for j in range(line):
        for way, place in enumerate((p, side, near, far)):
            arrived(slot(j, place, 1 - c), cs.at[j, way], cr.at[j, way])
    for copy in sends:
        copy.wait_send()


def gather_rows(line, residual, part, gain):
    dma = pltpu.SemaphoreType.DMA
    vmem = pl.BlockSpec(memory_space=pltpu.VMEM)
    _, half, features = part.shape
    return pl.pallas_call(
        functools.partial(gather_kernel, line),
        out_shape=(
            jax.ShapeDtypeStruct((half, features), jnp.bfloat16),
            jax.ShapeDtypeStruct((line * PLANE * 2, half, features), jnp.bfloat16),
        ),
        in_specs=[vmem] * 3,
        out_specs=(vmem, vmem),
        scratch_shapes=[
            pltpu.VMEM((half, features), jnp.bfloat16), dma, dma,
            dma((line,)), dma((line,)), dma((line, 3)), dma((line, 3)), dma((line, 4)), dma((line, 4)),
        ],
        compiler_params=pltpu.CompilerParams(
            collective_id=2, has_side_effects=True, vmem_limit_bytes=24 * 1024 * 1024
        ),
    )(residual, part, gain)


def scatter_kernel(
    line, terms, mixed, out, held, from_side, from_near, from_line,
    cs, cr, bs, br, as_, ar, zs, zr, fs, fr,
):
    s, c, z, p, near, side, far = places()
    to_near = (z * PLANE + near, c)
    to_side = (z * PLANE + side, c)
    to_core = (s, 1 - c)
    meet(
        [to_near, to_side, to_core]
        + [(((z + j) % line) * PLANE + p, c) for j in range(1, line)]
    )
    sends = []

    def send(*args):
        copy = remote(*args)
        copy.start()
        sends.append(copy)

    def arrived(block, send_sem, recv_sem):
        remote(block, block, send_sem, recv_sem, to_core).wait_recv()

    def add(a, b):
        return (a.astype(jnp.float32) + b.astype(jnp.float32)).astype(jnp.bfloat16)

    order = list(range(1, line)) + [0]
    for j in order:
        send(terms.at[(z + j) % line, :, 1 - c], held.at[j], cs.at[j], cr.at[j], to_core)

    def stage_core(j):
        arrived(held.at[j], cs.at[j], cr.at[j])
        zt = (z + j) % line
        for place in (side, far):
            held[j, place] = add(held[j, place], terms[zt, place, c])
        send(held.at[j, side], from_side.at[j, 0], bs.at[j, 0], br.at[j, 0], to_side)
        send(held.at[j, far], from_side.at[j, 1], bs.at[j, 1], br.at[j, 1], to_side)
        for place in (p, near):
            held[j, place] = add(held[j, place], terms[zt, place, c])

    def stage_side(j):
        arrived(from_side.at[j, 1], bs.at[j, 1], br.at[j, 1])
        held[j, near] = add(held[j, near], from_side[j, 1])
        send(held.at[j, near], from_near.at[j], as_.at[j], ar.at[j], to_near)
        arrived(from_side.at[j, 0], bs.at[j, 0], br.at[j, 0])
        held[j, p] = add(held[j, p], from_side[j, 0])

    def stage_near(j):
        arrived(from_near.at[j], as_.at[j], ar.at[j])
        held[j, p] = add(held[j, p], from_near[j])
        if j:
            send(
                held.at[j, p], from_line.at[j - 1], zs.at[j], zr.at[j],
                (((z + j) % line) * PLANE + p, c),
            )

    for step in range(line + 2):
        if step < line:
            stage_core(order[step])
        if 1 <= step <= line:
            stage_side(order[step - 1])
        if step >= 2:
            stage_near(order[step - 2])
    total = held[0, p].astype(jnp.float32)
    for j in range(1, line):
        arrived(from_line.at[j - 1], zs.at[j], zr.at[j])
        total = total + from_line[j - 1].astype(jnp.float32)
    out[c] = (mixed[...].astype(jnp.float32) + total).astype(jnp.bfloat16)
    send(out.at[c], out.at[c], fs, fr, to_core)
    arrived(out.at[1 - c], fs, fr)
    for copy in sends:
        copy.wait_send()


def scatter_sum(line, terms, mixed):
    dma = pltpu.SemaphoreType.DMA
    vmem = pl.BlockSpec(memory_space=pltpu.VMEM)
    half, features = mixed.shape
    block = (half, features)
    return pl.pallas_call(
        functools.partial(scatter_kernel, line),
        out_shape=jax.ShapeDtypeStruct((2,) + block, jnp.bfloat16),
        in_specs=[vmem] * 2,
        out_specs=vmem,
        scratch_shapes=[
            pltpu.VMEM((line, PLANE) + block, jnp.bfloat16),
            pltpu.VMEM((line, 2) + block, jnp.bfloat16),
            pltpu.VMEM((line,) + block, jnp.bfloat16),
            pltpu.VMEM((line - 1,) + block, jnp.bfloat16),
            dma((line,)), dma((line,)), dma((line, 2)), dma((line, 2)),
            dma((line,)), dma((line,)), dma((line,)), dma((line,)), dma, dma,
        ],
        compiler_params=pltpu.CompilerParams(
            collective_id=3, has_side_effects=True, vmem_limit_bytes=40 * 1024 * 1024
        ),
    )(terms, mixed)


def placed_body(
    residual, query_first, key_first, value_first, query_second, key_second, value_second,
    balance_first, balance_second, head_gain_first, head_gain_second, out_first, out_second,
    mlp_gain, up_weight, down_weight,
):
    tokens, line, wide = query_first.shape
    features = residual.shape[1]
    deep = value_second.shape[2]
    half = tokens // 2
    z = lax.axis_index("sp") // PLANE
    empty = jnp.zeros((tokens, line, wide - query_second.shape[2]), jnp.bfloat16)
    q = jnp.concatenate([query_first, query_second, empty], axis=-1).transpose(1, 0, 2)
    kv = jnp.concatenate([key_first, value_first, key_second, value_second], axis=-1)
    kv = kv.transpose(1, 0, 2)
    kv_all, q_all, up_all, down_all = exchange(line, kv, q, up_weight, down_weight)
    balance = jnp.stack([balance_first[z], balance_second[z]])
    heads = attention(
        line, wide // 2, query_second.shape[2] // 2, balance, q_all,
        kv_all.reshape(-1, kv.shape[2]), head_gain_first[None, :], head_gain_second[None, :],
    )
    heads = return_heads(line, heads)
    heads_first = heads[:, :, :wide].transpose(1, 0, 2).reshape(tokens, line * wide)
    heads_second = heads[:, :, wide:].transpose(1, 0, 2).reshape(tokens, line * deep)
    part = jnp.dot(heads_first, out_first, preferred_element_type=jnp.float32) + jnp.dot(
        heads_second, out_second, preferred_element_type=jnp.float32
    )
    part = part.astype(jnp.bfloat16).reshape(2, half, features)
    mixed, rows = gather_rows(line, residual.reshape(2, half, features), part, mlp_gain[None, :])
    up = up_all.reshape(-1, up_all.shape[2])
    down = down_all.reshape(-1, down_all.shape[2])
    lifted = jnp.dot(rows.reshape(-1, features), up, preferred_element_type=jnp.float32)
    active = jax.nn.relu(lifted)
    hidden = (active * active).astype(jnp.bfloat16)
    terms = last(hidden, down).astype(jnp.bfloat16)
    out = scatter_sum(line, terms.reshape(line, PLANE, 2, half, features), mixed)
    return out.reshape(tokens, features)


def placed(mesh):
    ranks = mesh.shape["sp"]
    cores = mesh.shape["tp"]
    return cores == 2 and ranks % PLANE == 0


def choose(mesh):
    ranks = mesh.shape["sp"]

    def run(*arrays):
        query_first, query_second, value_second, value_first = arrays[1], arrays[4], arrays[6], arrays[3]
        fits = (
            placed(mesh)
            and query_first.shape[1] * PLANE == ranks
            and query_second.shape[1] == query_first.shape[1]
            and value_first.shape[2] == query_first.shape[2] == 128
            and query_second.shape[2] + value_second.shape[2] == query_first.shape[2]
            and query_first.shape[0] % 32 == 0
            and arrays[14].shape[1] % (128 * ranks) == 0
        )
        return (placed_body if fits else body)(*arrays)

    return run


def solution(mesh):
    in_specs = (
        P("sp", None),
        P("sp", "tp", None),
        P("sp", "tp", None),
        P("sp", "tp", None),
        P("sp", "tp", None),
        P("sp", "tp", None),
        P("sp", "tp", None),
        P("tp"),
        P("tp"),
        P(),
        P(),
        P("tp", None),
        P("tp", None),
        P(),
        P("sp", "tp"),
        P("sp", "tp"),
    )
    out_specs = P("sp", None)
    return jax.shard_map(choose(mesh), mesh=mesh, in_specs=in_specs, out_specs=out_specs, check_vma=False)
```

profile of v0, /device:TPU:0, one launch (start us, length us, event | category | flops | bytes accessed | tf_op | source)
XLA Modules:
  0.0 233.6 jit_solution(7779241872035436652)
XLA Ops:
  0.0 1.4 dynamic_slice.7
  1.4 1.2 dynamic_slice.6
  2.6 1.3 pad_maximum_fusion.balance
  4.0 1.6 copy.27
  5.6 0.9 copy.23
  6.5 1.6 copy.24
  8.1 1.6 copy.28
  9.7 1.0 maximum_bitcast_fusion.1.q
  10.7 1.6 copy.25
  12.3 1.6 copy.26
  13.9 1.1 maximum_bitcast_fusion.kv
  15.1 1.2 copy-done.4
  16.3 52.4 %shard_map.154 = (bf16[16,128,384]{2,1,0:T(8,128)(2,1)S(1)}, bf16[4,128,256]{2,1,0:T(8,128)(2,1)S(1)}, bf16[16,128,256]{2,1,0:T(8,128)(2,1)S(1)}, bf16[16,128,256]{2,1,0:T(8,128)(2,1)S(1)}) custom-call(bf16[4,128,384]{2,1,0:T(8,128)(2,1)S(1)} %maximum_bitcast_fusion.kv, bf16[4,128,256]{2,1,0:T(8,128)(2,1)S(1)} %maximum_bitcast_fusion.1.q, ...), custom_call_target="tpu_custom_call" | custom-call | tf_op jit(solution)/shard_map/pallas_call | solution.py:237
  68.7 1.0 copy-done.10
  69.7 1.0 copy-done.11
  70.7 6.8 %shard_map.155.heads = bf16[4,128,192]{2,1,0:T(8,128)(2,1)S(1)} custom-call(f32[2]{0:T(128)S(1)} %pad_maximum_fusion.balance, bf16[4,128,256]{2,1,0:T(8,128)(2,1)S(1)} %get-tuple-element.11.q, bf16[2048,384]{1,0:T(8,128)(2,1)S(1)} %bitcast.31, f32[1,128]{1,0:T(1,128)S(1)} %bitcast.34, f32[1,64]{1,0:T(1,128)S(1)} %bitcast.35), custom_call_target="tpu_custom_call" | custom-call | tf_op jit(solution)/shard_map/pallas_call | solution.py:304
  78.2 26.3 %shard_map.156 = bf16[4,128,192]{2,1,0:T(8,128)(2,1)} custom-call(bf16[4,128,192]{2,1,0:T(8,128)(2,1)} %copy-done.2), custom_call_target="tpu_custom_call" | custom-call | tf_op jit(solution)/shard_map/pallas_call | solution.py:335
  104.5 0.9 slice_bitcast_fusion
  106.5 1.6 fusion.5
  109.2 47.6 %shard_map.157 = (bf16[64,2048]{1,0:T(8,128)(2,1)S(1)}, bf16[32,64,2048]{2,1,0:T(8,128)(2,1)S(1)}) custom-call(bf16[2,64,2048]{2,1,0:T(8,128)(2,1)S(1)} %bitcast.32, bf16[2,64,2048]{2,1,0:T(8,128)(2,1)S(1)} %bitcast.30, f32[1,2048]{1,0:T(1,128)S(1)} %bitcast.33), custom_call_target="tpu_custom_call" | custom-call | tf_op jit(solution)/shard_map/pallas_call | solution.py:408
  156.8 3.2 %copy-done.9 = bf16[32,64,2048]{2,1,0:T(8,128)(2,1)} copy-done((bf16[32,64,2048]{2,1,0:T(8,128)(2,1)}, bf16[32,64,2048]{2,1,0:T(8,128)(2,1)S(1)}, u32[]{:S(2)}) %copy-start.9) | copy-done | bytes 8388632
  160.0 13.4 %convolution_convert_fusion = bf16[2048,2048]{1,0:T(8,128)(2,1)} fusion(bf16[2048,256]{1,0:T(8,128)(2,1)} %bitcast.38, bf16[2048,2048]{1,0:T(8,128)(2,1)} %bitcast.36, bf16[2048,256]{1,0:T(8,128)(2,1)} %bitcast.37), kind=kOutput, calls=%fused_computation | convolution fusion | flops 4300734464 | bytes 18874368 | tf_op jit(solution)/shard_map/dot_general | solution.py:258
  173.4 3.4 %copy-done.1 = bf16[2048,2048]{1,0:T(8,128)(2,1)S(1)} copy-done((bf16[2048,2048]{1,0:T(8,128)(2,1)S(1)}, bf16[2048,2048]{1,0:T(8,128)(2,1)}, u32[]{:S(2)}) %copy-start.1) | copy-done | bytes 8388632
  176.8 55.9 %shard_map.158 = bf16[2,64,2048]{2,1,0:T(8,128)(2,1)S(1)} custom-call(bf16[4,4,2,64,2048]{4,3,2,1,0:T(8,128)(2,1)S(1)} %bitcast.28, bf16[64,2048]{1,0:T(8,128)(2,1)S(1)} %get-tuple-element.16.mixed), custom_call_target="tpu_custom_call" | custom-call | tf_op jit(solution)/shard_map/pallas_call | solution.py:504
  (26 shorter events, 3.8 us)
Async XLA Ops:
  0.0 108.1 %copy-start = (bf16[512,2048]{1,0:T(8,128)(2,1)S(1)}, bf16[512,2048]{1,0:T(8,128)(2,1)}, u32[]{:S(2)}) copy-start(bf16[512,2048]{1,0:T(8,128)(2,1)} %param.27) | copy-start | bytes 6291460
  0.0 15.1 %copy-start.3 = (bf16[128,4096]{1,0:T(8,128)(2,1)S(1)}, bf16[128,4096]{1,0:T(8,128)(2,1)}, u32[]{:S(2)}) copy-start(bf16[128,4096]{1,0:T(8,128)(2,1)} %up.1) | copy-start | bytes 3145732
  10.7 60.0 %copy-start.7 = (f32[128]{0:T(128)S(1)}, f32[128]{0:T(128)}, u32[]{:S(2)}) copy-start(f32[128]{0:T(128)} %param.25) | copy-start | bytes 1540
  10.7 60.0 %copy-start.8 = (f32[64]{0:T(128)S(1)}, f32[64]{0:T(128)}, u32[]{:S(2)}) copy-start(f32[64]{0:T(128)} %param.26) | copy-start | bytes 772
  15.1 1.2 copy-start.4
  68.7 1.0 copy-start.10
  69.7 1.0 copy-start.11
  77.5 0.7 copy-start.2
  108.1 1.0 copy-start.5
  108.1 1.0 copy-start.6
  156.8 3.2 %copy-start.9 = (bf16[32,64,2048]{2,1,0:T(8,128)(2,1)}, bf16[32,64,2048]{2,1,0:T(8,128)(2,1)S(1)}, u32[]{:S(2)}) copy-start(bf16[32,64,2048]{2,1,0:T(8,128)(2,1)S(1)} %get-tuple-element.13) | copy-start | bytes 25165828
  173.4 3.4 %copy-start.1 = (bf16[2048,2048]{1,0:T(8,128)(2,1)S(1)}, bf16[2048,2048]{1,0:T(8,128)(2,1)}, u32[]{:S(2)}) copy-start(bf16[2048,2048]{1,0:T(8,128)(2,1)} %convolution_convert_fusion) | copy-start | bytes 25165828
where the time goes:
time: 234 us
  Pallas kernels  189 us (81%)
  local copies, waits for them, and re-layouts  25.5 us (11%)
  matrix products  15.5 us (7%)
  other arithmetic  3.45 us (1%)
    pallas_call x1, Pallas kernels, scatter_sum(): pl.pallas_call(functools.partial(scatter_kernel, line), out_shape=jax.Sha...  55.9 us
    pallas_call x1, Pallas kernels, exchange(): pl.pallas_call(functools.partial(exchange_kernel, line), out_shape=(jax.S...  52.4 us
    pallas_call x1, Pallas kernels, gather_rows(): pl.pallas_call(functools.partial(gather_kernel, line), out_shape=(jax.Sha...  47.6 us
    pallas_call x1, Pallas kernels, return_heads(): pl.pallas_call(functools.partial(return_kernel, line), out_shape=jax.Shap...  26.3 us
    unnamed x31, local copies, waits for them, and re-layouts  20.7 us
    dot_general x1, matrix products, last(): lax.dot_general(a, b, (((1,), (1,)), ((), ())), preferred_element_type=jn...  13.4 us
    pallas_call x1, Pallas kernels, attention(): pl.pallas_call(functools.partial(attention_kernel, line, size_a, size_b),...  6.77 us

commit v1 on v0

v1 whole, which is shorter than its diff:
```python
import functools
import math

import jax
import jax.numpy as jnp
from jax import lax
from jax.experimental import pallas as pl
from jax.experimental.pallas import tpu as pltpu
from jax.sharding import PartitionSpec as P

DK_A = 64
DK_B = 32


EPSILON = 1e-06
HEAD_SCALE = 0.8


def attend(queries, keys, values, balance, gain, device, head_size):
    tokens = queries.shape[0]
    heads = queries.shape[1]
    seq = keys.shape[0]
    depth = values.shape[2]
    block = math.gcd(512, seq)
    scale = head_size ** (-0.5)
    query_maps = queries.reshape(tokens, heads, 2, head_size)
    key_maps = keys.reshape(seq, heads, 2, head_size)
    first_row = device * tokens
    positions = first_row + jnp.arange(tokens, dtype=jnp.int32)
    needed = (first_row + tokens + block - 1) // block

    def block_scores(number):
        start = number * block
        key_block = lax.dynamic_slice_in_dim(key_maps, start, block, 0)
        scores = (
            jnp.einsum("qhmd,khmd->hmqk", query_maps, key_block, preferred_element_type=jnp.float32)
            * scale
        )
        columns = start + jnp.arange(block, dtype=jnp.int32)
        visible = columns[None, :] <= positions[:, None]
        return (jnp.where(visible, scores, -jnp.inf), start)

    def statistics(number, carry):
        highest, total = carry
        scores, start = block_scores(number)
        fresh = jnp.maximum(highest, jnp.max(scores, axis=-1, keepdims=True))
        total = total * jnp.exp(highest - fresh) + jnp.sum(
            jnp.exp(scores - fresh), axis=-1, keepdims=True
        )
        return (fresh, total)

    start_high = jnp.full((heads, 2, tokens, 1), -jnp.inf, jnp.float32)
    start_total = jnp.zeros((heads, 2, tokens, 1), jnp.float32)
    highest, total = lax.fori_loop(0, needed, statistics, (start_high, start_total))

    def accumulate(number, result):
        scores, start = block_scores(number)
        probs = jnp.exp(scores - highest) / total
        mixed = (probs[:, 0] - balance[:, None, None] * probs[:, 1]).astype(jnp.bfloat16)
        value_block = lax.dynamic_slice_in_dim(values, start, block, 0)
        return result + jnp.einsum(
            "hqk,khe->qhe", mixed, value_block, preferred_element_type=jnp.float32
        )

    summed = lax.fori_loop(0, needed, accumulate, jnp.zeros((tokens, heads, depth), jnp.float32))
    power = jnp.mean(summed * summed, axis=-1, keepdims=True)
    normed = summed * lax.rsqrt(power + EPSILON) * gain * HEAD_SCALE
    return normed.astype(jnp.bfloat16).reshape(tokens, heads * depth)


def body(
    residual,
    query_first,
    key_first,
    value_first,
    query_second,
    key_second,
    value_second,
    balance_first,
    balance_second,
    head_gain_first,
    head_gain_second,
    out_first,
    out_second,
    mlp_gain,
    up_weight,
    down_weight,
):
    device = lax.axis_index("sp")
    keys_first, values_first, keys_second, values_second = (
        lax.all_gather(key_first, "sp", axis=0, tiled=True),
        lax.all_gather(value_first, "sp", axis=0, tiled=True),
        lax.all_gather(key_second, "sp", axis=0, tiled=True),
        lax.all_gather(value_second, "sp", axis=0, tiled=True),
    )
    heads_first = attend(
        query_first, keys_first, values_first, balance_first, head_gain_first, device, DK_A
    )
    heads_second = attend(
        query_second, keys_second, values_second, balance_second, head_gain_second, device, DK_B
    )
    head_term = jnp.dot(heads_first, out_first, preferred_element_type=jnp.float32) + jnp.dot(
        heads_second, out_second, preferred_element_type=jnp.float32
    )
    head_total = lax.psum(head_term.astype(jnp.bfloat16), "tp").astype(jnp.float32)
    mixed = (residual.astype(jnp.float32) + head_total).astype(jnp.bfloat16)
    mixed_float = mixed.astype(jnp.float32)
    power = jnp.mean(mixed_float * mixed_float, axis=-1, keepdims=True)
    normed = (mixed_float * lax.rsqrt(power + EPSILON) * mlp_gain).astype(jnp.bfloat16)
    up_whole, down_whole = (
        lax.all_gather(up_weight, "sp", axis=0, tiled=True),
        lax.all_gather(down_weight, "sp", axis=0, tiled=True),
    )
    lifted = jnp.dot(normed, up_whole, preferred_element_type=jnp.float32)
    active = jax.nn.relu(lifted)
    hidden = (active * active).astype(jnp.bfloat16)
    down_term = lax.dot_general(
        hidden, down_whole, (((1,), (1,)), ((), ())), preferred_element_type=jnp.float32
    )
    added = lax.psum(down_term.astype(jnp.bfloat16), "tp").astype(jnp.float32)
    return (mixed_float + added).astype(jnp.bfloat16)


PLANE = 4
MESH = pl.DeviceIdType.MESH


def remote(src, dst, send_sem, recv_sem, device):
    return pltpu.make_async_remote_copy(
        src_ref=src, dst_ref=dst, send_sem=send_sem, recv_sem=recv_sem,
        device_id=device, device_id_type=MESH,
    )


def last(a, b):
    return lax.dot_general(a, b, (((1,), (1,)), ((), ())), preferred_element_type=jnp.float32)


def add(a, b):
    return (a.astype(jnp.float32) + b.astype(jnp.float32)).astype(jnp.bfloat16)


def layer_kernel(
    line, size_a, size_b,
    bal_a, bal_b, resid_h, q1_h, k1_h, v1_h, q2_h, k2_h, v2_h, gain_a, gain_b, o1_h, o2_h,
    mlp_gain, up_h, down_h,
    out,
    resid, q1, k1, v1, q2, k2, v2, o1, o2, kv_own, q_own, kv_all, q_all, heads_out, heads_in,
    up_all, down_all, part, other_part, mixed, rows, hidden, terms, held, acc, below, above, total,
    fetch, kzs, kzr, qzs, qzr, kps, kpr, uzs, uzr, ups, upr, dzs, dzr, dps, dpr, hzs, hzr,
    sws, swr, rus, rds, rr, rcs, rcr, ts, tr, cus, cds, cbr, car, fs, fr,
):
    s = lax.axis_index("sp")
    c = lax.axis_index("tp")
    z = s // PLANE
    p = s % PLANE
    x = p % 2
    y = p // 2
    flip_x = y * 2 + 1 - x
    flip_y = (1 - y) * 2 + x
    near = (1 - c) * flip_x + c * flip_y
    side = (1 - c) * flip_y + c * flip_x
    far = (1 - y) * 2 + 1 - x
    to_near = (z * PLANE + near, c)
    to_side = (z * PLANE + side, c)
    to_core = (s, 1 - c)
    to_up = (s + PLANE, c)
    to_down = (s - PLANE, c)

    tokens = kv_own.shape[1]
    wide = gain_a.shape[1]
    deep = gain_b.shape[1]
    features = resid.shape[1]
    span = PLANE * tokens
    depth = up_h.shape[0]
    width = up_all.shape[1]
    half = tokens // 2
    piece = PLANE * depth

    def fetched(number, src, dst):
        return pltpu.make_async_copy(src, dst, fetch.at[number])

    def at_place(ref, number, size):
        return ref.at[pl.ds(pl.multiple_of(number * size, size), size)]

    def columns(ref, number):
        return ref.at[:, pl.ds(pl.multiple_of(number * width, width), width)]

    small = [
        fetched(0, k1_h, k1), fetched(1, v1_h, v1), fetched(2, k2_h, k2), fetched(3, v2_h, v2),
        fetched(4, q1_h, q1), fetched(5, q2_h, q2),
    ]
    own_up = fetched(6, columns(up_h, z), at_place(up_all, s, depth))
    own_down = fetched(7, columns(down_h, z), at_place(down_all, s, depth))
    large = [fetched(8, resid_h, resid), fetched(9, o1_h, o1), fetched(10, o2_h, o2)]
    for copy in small + [own_up, own_down] + large:
        copy.start()

    barrier = pltpu.get_barrier_semaphore()
    peers = [to_near, to_side, to_core] + [(((z + j) % line) * PLANE + p, c) for j in range(1, line)]
    for device in peers:
        pl.semaphore_signal(barrier, inc=1, device_id=device, device_id_type=MESH)

    sends = []

    def send(*args):
        copy = remote(*args)
        copy.start()
        sends.append((None, copy))

    def send_if(condition, *args):
        copy = remote(*args)

        @pl.when(condition)
        def _():
            copy.start()

        sends.append((condition, copy))

    def arrived(block, sem):
        remote(block, block, fs.at[0], sem, to_core).wait_recv()

    for copy in small:
        copy.wait()
    count = tokens * line
    order = lax.broadcasted_iota(jnp.int32, (count, count), 0)
    place = lax.broadcasted_iota(jnp.int32, (count, count), 1)
    pick = jnp.where(place == (order % tokens) * line + order // tokens, 1.0, 0.0).astype(jnp.bfloat16)

    def by_head(value):
        moved = jnp.dot(pick, value, preferred_element_type=jnp.float32).astype(jnp.bfloat16)
        return moved.reshape(line, tokens, value.shape[1])

    kv_own[:, :, 0:wide] = by_head(k1[...])
    kv_own[:, :, wide:2 * wide] = by_head(v1[...])
    kv_own[:, :, 2 * wide:3 * wide] = by_head(jnp.concatenate([k2[...], v2[...]], axis=1))
    q_own[:, :, 0:wide] = by_head(q1[...])
    q_own[:, :, wide:] = by_head(q2[...])
    pl.semaphore_wait(barrier, len(peers))

    def ahead(j):
        return (z + j) % line

    def behind(j):
        return (z + line - j) % line

    def z_peer(j):
        return (ahead(j) * PLANE + p, c)

    mine = at_place(kv_all, s, tokens)
    for j in range(1, line):
        send(kv_own.at[ahead(j)], mine, kzs.at[j], kzr.at[j], z_peer(j))
    send(kv_own.at[z], mine, kps.at[0, 0], kpr.at[0, 0], to_near)
    send(kv_own.at[z], mine, kps.at[0, 1], kpr.at[0, 1], to_side)
    for j in range(1, line):
        send(q_own.at[ahead(j)], q_all.at[z], qzs.at[j], qzr.at[j], z_peer(j))
    mine[...] = kv_own[z]
    q_all[z] = q_own[z]

    weights = {
        "up": (up_h, up_all, own_up, uzs, uzr, ups, upr),
        "down": (down_h, down_all, own_down, dzs, dzr, dps, dpr),
    }

    def along(name, j):
        source, whole, _, ss, sr, _, _ = weights[name]
        send(columns(source, ahead(j)), at_place(whole, s, depth), ss.at[j], sr.at[j], z_peer(j))

    def spread(name, j):
        _, whole, own, _, sr, ss, rr_ = weights[name]
        block = at_place(whole, behind(j) * PLANE + p, depth)
        if j:
            arrived(block, sr.at[j])
        else:
            own.wait()
        send(block, block, ss.at[j, 0], rr_.at[j, 0], to_near)
        send(block, block, ss.at[j, 1], rr_.at[j, 1], to_side)

    def relay(name, j):
        _, whole, _, _, _, ss, rr_ = weights[name]
        block = at_place(whole, behind(j) * PLANE + near, depth)
        arrived(block, rr_.at[j, 0])
        send(block, block, ss.at[j, 2], rr_.at[j, 2], to_side)

    def settle(name, j):
        _, whole, _, _, _, _, rr_ = weights[name]
        for way, where in ((1, side), (2, far)):
            arrived(at_place(whole, behind(j) * PLANE + where, depth), rr_.at[j, way])

    def kv_spread(j):
        block = at_place(kv_all, behind(j) * PLANE + p, tokens)
        arrived(block, kzr.at[j])
        send(block, block, kps.at[j, 0], kpr.at[j, 0], to_near)
        send(block, block, kps.at[j, 1], kpr.at[j, 1], to_side)

    def kv_relay(j):
        block = at_place(kv_all, behind(j) * PLANE + near, tokens)
        arrived(block, kpr.at[j, 0])
        send(block, block, kps.at[j, 2], kpr.at[j, 2], to_side)

    for j in range(1, line):
        along("up", j)
    kv_spread(1)
    kv_relay(0)
    kv_spread(2)
    kv_relay(1)
    kv_spread(3)
    kv_relay(2)
    kv_relay(3)
    spread("up", 0)
    for j in range(line):
        for way, where in ((1, side), (2, far)):
            arrived(at_place(kv_all, behind(j) * PLANE + where, tokens), kpr.at[j, way])
    for j in range(1, line):
        arrived(q_all.at[behind(j)], qzr.at[j])

    lanes_a = lax.broadcasted_iota(jnp.int32, (tokens, wide), 1)
    lanes_b = lax.broadcasted_iota(jnp.int32, (tokens, deep), 1)
    line_rows = lax.broadcasted_iota(jnp.int32, (tokens, span), 0) + p * tokens
    visible = lax.broadcasted_iota(jnp.int32, (tokens, span), 1) <= line_rows

    def mix(queries, lanes, keys_at, values_at, size, b, keys_number):
        maps = []
        for m in range(2):
            chosen = (lanes >= m * size) & (lanes < (m + 1) * size)
            picked = jnp.where(chosen, queries, jnp.zeros_like(queries))
            scores = last(picked, kv_all[0:keys_number, keys_at]) * size ** (-0.5)
            tail_scores = jnp.where(visible, scores[:, keys_number - span:], -jnp.inf)
            if keys_number > span:
                scores = jnp.concatenate([scores[:, : keys_number - span], tail_scores], axis=1)
            else:
                scores = tail_scores
            powers = jnp.exp(scores - jnp.max(scores, axis=-1, keepdims=True))
            maps.append((powers, jnp.sum(powers, axis=-1, keepdims=True)))
        (e1, l1), (e2, l2) = maps
        mixing = (e1 * (1.0 / l1) - e2 * (b / l2)).astype(jnp.bfloat16)
        return jnp.dot(mixing, kv_all[0:keys_number, values_at], preferred_element_type=jnp.float32)

    def norm(value, gain):
        power = jnp.mean(value * value, axis=-1, keepdims=True)
        return (value * lax.rsqrt(power + EPSILON) * gain[...] * HEAD_SCALE).astype(jnp.bfloat16)

    def tile(j):
        number = (j + 1) * span
        first = mix(
            q_all[j, :, 0:wide], lanes_a, slice(0, wide), slice(wide, 2 * wide), size_a, bal_a[z], number
        )
        heads_out[j, :, 0:wide] = norm(first, gain_a)
        second = mix(
            q_all[j, :, wide:], lanes_b, slice(2 * wide, 2 * wide + deep),
            slice(2 * wide, 3 * wide), size_b, bal_b[z], number,
        )
        heads_out[j, :, wide:] = norm(second[:, wide - deep:wide], gain_b)
        send_if(j != z, heads_out.at[j], heads_in.at[z], hzs.at[j], hzr.at[z], (j * PLANE + p, c))

    tile(3)
    relay("up", 0)
    tile(2)
    spread("up", 1)
    tile(1)
    tile(0)
    heads_in[z] = heads_out[z]
    along("down", 1)
    along("down", 2)
    relay("up", 1)
    spread("up", 2)
    relay("up", 2)
    spread("up", 3)
    spread("down", 0)
    for copy in large:
        copy.wait()
    for h in range(line):
        block = heads_in.at[h]

        @pl.when(h != z)
        def _():
            arrived(block, hzr.at[h])

    heads_first = jnp.concatenate([heads_in[h, :, 0:wide] for h in range(line)], axis=1)
    heads_second = jnp.concatenate([heads_in[h, :, wide:] for h in range(line)], axis=1)
    step = features // 4
    for n in range(4):
        at = slice(n * step, (n + 1) * step)
        value = jnp.dot(heads_first, o1[:, at], preferred_element_type=jnp.float32) + jnp.dot(
            heads_second, o2[:, at], preferred_element_type=jnp.float32
        )
        part[:, :, at] = value.astype(jnp.bfloat16).reshape(2, half, step)
    swap = remote(part.at[1 - c], other_part, sws.at[0], swr.at[0], to_core)
    swap.start()
    relay("up", 3)
    swap.wait()
    both = part[c].astype(jnp.float32) + other_part[...].astype(jnp.float32)
    mine_rows = pl.ds(pl.multiple_of(c * half, half), half)
    mixed[...] = (resid[mine_rows, :].astype(jnp.float32) + both).astype(jnp.bfloat16)
    whole = mixed[...].astype(jnp.float32)
    power = jnp.mean(whole * whole, axis=-1, keepdims=True)
    own_slot = at_place(rows, z * 2 + c, half)
    own_slot[...] = (whole * lax.rsqrt(power + EPSILON) * mlp_gain[...]).astype(jnp.bfloat16)

    send_if(z < line - 1, own_slot, own_slot, rus.at[0], rr.at[z], to_up)
    send_if(z > 0, own_slot, own_slot, rds.at[0], rr.at[z], to_down)
    send(own_slot, own_slot, rcs.at[0], rcr.at[z], to_core)
    relay("down", 0)
    for d in range(1, line):
        from_low = at_place(rows, jnp.maximum(z - d, 0) * 2 + c, half)
        low = jnp.maximum(z - d, 0)

        @pl.when(z >= d)
        def _():
            arrived(from_low, rr.at[low])

        send_if((z >= d) & (z < line - 1), from_low, from_low, rus.at[d], rr.at[low], to_up)
        send_if(z >= d, from_low, from_low, rcs.at[d], rcr.at[low], to_core)
        high = jnp.minimum(z + d, line - 1)
        from_high = at_place(rows, high * 2 + c, half)

        @pl.when(z + d < line)
        def _():
            arrived(from_high, rr.at[high])

        send_if((z + d < line) & (z > 0), from_high, from_high, rds.at[d], rr.at[high], to_down)
        send_if(z + d < line, from_high, from_high, rcs.at[line - 1 + d], rcr.at[high], to_core)
        if d == 1:
            along("down", 3)
            spread("down", 1)
        if d == 2:
            relay("down", 1)
            spread("down", 2)
    for k in range(line):
        arrived(at_place(rows, k * 2 + 1 - c, half), rcr.at[k])
    for j in range(line):
        settle("up", j)
    relay("down", 2)

    lift = 256

    @pl.loop(0, width // lift)
    def _(n):
        at = pl.ds(pl.multiple_of(n * lift, lift), lift)
        lifted = jnp.maximum(jnp.dot(rows[...], up_all[:, at], preferred_element_type=jnp.float32), 0.0)
        hidden[:, at] = (lifted * lifted).astype(jnp.bfloat16)

    spread("down", 3)
    relay("down", 3)
    for j in range(line):
        settle("down", j)

    def chunk(k):
        at = slice(k * piece, (k + 1) * piece)
        value = last(hidden[...], down_all[k * piece:(k + 1) * piece, :]).astype(jnp.bfloat16)
        terms[:, :, :, at] = value.reshape(line, 2, half, piece)
        send(terms.at[:, 1 - c, :, at], held.at[:, :, at], ts.at[k], tr.at[k], to_core)

    def reduce(k):
        at = slice(k * piece, (k + 1) * piece)
        arrived(held.at[:, :, at], tr.at[k])
        for zd in range(line):
            acc[zd, :, at] = add(terms[zd, c, :, at], held[zd, :, at])
        for d in range(line - 1, 0, -1):
            high = jnp.minimum(z + d, line - 1)
            block = below.at[high, :, at]

            @pl.when((z + d < line) & (z > 0))
            def _():
                arrived(block, cbr.at[high, k])
                acc[high, :, at] = add(acc[high, :, at], below[high, :, at])

            send_if(z + d < line, acc.at[high, :, at], block, cus.at[d, k], cbr.at[high, k], to_up)
            low = jnp.maximum(z - d, 0)
            block = above.at[low, :, at]

            @pl.when((z >= d) & (z < line - 1))
            def _():
                arrived(block, car.at[low, k])
                acc[low, :, at] = add(acc[low, :, at], above[low, :, at])

            send_if(z >= d, acc.at[low, :, at], block, cds.at[d, k], car.at[low, k], to_down)

    def finish(k):
        at = slice(k * piece, (k + 1) * piece)
        total[...] = mixed[:, at].astype(jnp.float32) + acc[z, :, at].astype(jnp.float32)

        @pl.when(z > 0)
        def _():
            arrived(below.at[z, :, at], cbr.at[z, k])
            total[...] += below[z, :, at].astype(jnp.float32)

        @pl.when(z < line - 1)
        def _():
            arrived(above.at[z, :, at], car.at[z, k])
            total[...] += above[z, :, at].astype(jnp.float32)

        out[c, :, at] = total[...].astype(jnp.bfloat16)
        send(out.at[c, :, at], out.at[c, :, at], fs.at[k], fr.at[k], to_core)

    for k in range(line):
        chunk(k)
        if k:
            reduce(k - 1)
    reduce(line - 1)
    for k in range(line):
        finish(k)
    for k in range(line):
        at = slice(k * piece, (k + 1) * piece)
        arrived(out.at[1 - c, :, at], fr.at[k])
    for condition, copy in sends:
        if condition is None:
            copy.wait_send()
        else:

            @pl.when(condition)
            def _():
                copy.wait_send()


def layer(
    line, residual, q1, k1, v1, q2, k2, v2, bal_a, bal_b, gain_a, gain_b, o1, o2, mlp_gain, up, down
):
    tokens, features = residual.shape
    half = tokens // 2
    wide = v1.shape[1]
    deep = v2.shape[1]
    n = line * PLANE
    width = up.shape[1] // line
    depth = up.shape[0]
    b16 = jnp.bfloat16
    dma = pltpu.SemaphoreType.DMA
    vmem = pl.BlockSpec(memory_space=pltpu.VMEM)
    smem = pl.BlockSpec(memory_space=pltpu.SMEM)
    any_ = pl.BlockSpec(memory_space=pl.ANY)

    def buffer(*shape):
        return pltpu.VMEM(shape, b16)

    return pl.pallas_call(
        functools.partial(layer_kernel, line, q1.shape[1] // 2, q2.shape[1] // 2),
        out_shape=jax.ShapeDtypeStruct((2, half, features), b16),
        in_specs=[smem, smem] + [any_] * 7 + [vmem, vmem, any_, any_, vmem, any_, any_],
        out_specs=vmem,
        scratch_shapes=[
            buffer(tokens, features), buffer(*q1.shape), buffer(*k1.shape), buffer(*v1.shape),
            buffer(*q2.shape), buffer(*k2.shape), buffer(*v2.shape), buffer(*o1.shape), buffer(*o2.shape),
            buffer(line, tokens, 3 * wide), buffer(line, tokens, wide + deep),
            buffer(n * tokens, 3 * wide), buffer(line, tokens, wide + deep),
            buffer(line, tokens, wide + deep), buffer(line, tokens, wide + deep),
            buffer(n * depth, width), buffer(n * depth, width),
            buffer(2, half, features), buffer(half, features), buffer(half, features),
            buffer(line * tokens, features), buffer(line * tokens, width),
            buffer(line, 2, half, features), buffer(line, half, features), buffer(line, half, features),
            buffer(line, half, features), buffer(line, half, features),
            pltpu.VMEM((half, PLANE * depth), jnp.float32),
            dma((11,)),
            dma((line,)), dma((line,)), dma((line,)), dma((line,)), dma((line, 3)), dma((line, 3)),
            dma((line,)), dma((line,)), dma((line, 3)), dma((line, 3)),
            dma((line,)), dma((line,)), dma((line, 3)), dma((line, 3)),
            dma((line,)), dma((line,)), dma((1,)), dma((1,)),
            dma((line,)), dma((line,)), dma((line,)), dma((2 * line - 1,)), dma((line,)),
            dma((line,)), dma((line,)), dma((line, line)), dma((line, line)),
            dma((line, line)), dma((line, line)), dma((line,)), dma((line,)),
        ],
        compiler_params=pltpu.CompilerParams(
            collective_id=0, has_side_effects=True, vmem_limit_bytes=60 * 1024 * 1024
        ),
    )(bal_a, bal_b, residual, q1, k1, v1, q2, k2, v2, gain_a, gain_b, o1, o2, mlp_gain, up, down)


def placed_body(
    residual, query_first, key_first, value_first, query_second, key_second, value_second,
    balance_first, balance_second, head_gain_first, head_gain_second, out_first, out_second,
    mlp_gain, up_weight, down_weight,
):
    tokens, line, _ = query_first.shape

    def flat(array):
        return array.reshape(tokens * line, array.shape[2])

    out = layer(
        line, residual, flat(query_first), flat(key_first), flat(value_first), flat(query_second),
        flat(key_second), flat(value_second), balance_first, balance_second,
        head_gain_first[None, :], head_gain_second[None, :], out_first, out_second,
        mlp_gain[None, :], up_weight, down_weight,
    )
    return out.reshape(residual.shape)


def placed(mesh):
    ranks = mesh.shape["sp"]
    cores = mesh.shape["tp"]
    return cores == 2 and ranks % PLANE == 0


def choose(mesh):
    ranks = mesh.shape["sp"]

    def run(*arrays):
        query_first, query_second, value_second, value_first = arrays[1], arrays[4], arrays[6], arrays[3]
        fits = (
            placed(mesh)
            and query_first.shape[1] * PLANE == ranks
            and query_second.shape[1] == query_first.shape[1]
            and value_first.shape[2] == query_first.shape[2] == 128
            and query_second.shape[2] + value_second.shape[2] == query_first.shape[2]
            and query_first.shape[0] % 32 == 0
            and arrays[14].shape[1] % (128 * ranks) == 0
        )
        return (placed_body if fits else body)(*arrays)

    return run


def solution(mesh):
    in_specs = (
        P("sp", None),
        P("sp", "tp", None),
        P("sp", "tp", None),
        P("sp", "tp", None),
        P("sp", "tp", None),
        P("sp", "tp", None),
        P("sp", "tp", None),
        P("tp"),
        P("tp"),
        P(),
        P(),
        P("tp", None),
        P("tp", None),
        P(),
        P("sp", "tp"),
        P("sp", "tp"),
    )
    out_specs = P("sp", None)
    return jax.shard_map(choose(mesh), mesh=mesh, in_specs=in_specs, out_specs=out_specs, check_vma=False)
```

time: 234 us -> 144 us (0.62)
  Pallas kernels: 189 us -> 137 us
  local copies, waits for them, and re-layouts: 25.5 us -> 6.71 us
  matrix products: 15.5 us -> 0 us
  other arithmetic: 3.45 us -> 0 us
    pallas_call x5 -> x1, Pallas kernels: 189 us -> 137 us  [layer(): pl.pallas_call(functools.partial(layer_kernel, line, q1.shape[1] // 2, q2...]
    dot_general x3 -> x0, matrix products: 15.5 us -> none  [the longest x1 13.4 us: last(): lax.dot_general(a, b, (((1,), (1,)), ((), ())), preferred_element_type=jn...]
    unnamed x31 -> x4, local copies, waits for them, and re-layouts: 20.7 us -> 6.71 us
    dynamic_slice x2 -> x0, local copies, waits for them, and re-layouts: 2.63 us -> none  [placed_body(): balance = jnp.stack([balance_first[z], balance_second[z]])]
where the time goes in v1:
time: 144 us
  Pallas kernels  137 us (95%)
  local copies, waits for them, and re-layouts  6.71 us (5%)
    pallas_call x1, Pallas kernels, layer(): pl.pallas_call(functools.partial(layer_kernel, line, q1.shape[1] // 2, q2...  137 us
    unnamed x4, local copies, waits for them, and re-layouts  6.71 us

profile of v1, /device:TPU:0, one launch (start us, length us, event | category | flops | bytes accessed | tf_op | source)
XLA Modules:
  0.0 143.7 jit_solution(5389226209598207786)
XLA Ops:
  0.0 1.6 %copy.17 = bf16[128,4,64]{2,1,0:T(4,128)(2,1)} copy(bf16[128,4,64]{0,2,1:T(8,128)(2,1)} %param.20) | data formatting | bytes 131072 | tf_op args[4]
  1.6 1.6 %copy.18 = bf16[128,4,64]{2,1,0:T(4,128)(2,1)} copy(bf16[128,4,64]{0,2,1:T(8,128)(2,1)} %param.21) | data formatting | bytes 131072 | tf_op args[5]
  3.2 1.6 %copy.19 = bf16[128,4,64]{2,1,0:T(4,128)(2,1)} copy(bf16[128,4,64]{0,2,1:T(8,128)(2,1)} %param.22) | data formatting | bytes 131072 | tf_op args[6]
  4.8 136.9 %shard_map.154 = bf16[2,64,2048]{2,1,0:T(8,128)(2,1)} custom-call(f32[4]{0:T(128)} %bal_a.1, f32[4]{0:T(128)} %bal_b.1, bf16[128,2048]{1,0:T(8,128)(2,1)} %resid_h.1, bf16[512,128]{1,0:T(8,128)(2,1)} %bitcast.14, bf16[512,128]{1,0:T(8,128)(2,1)} %bitcast.15, bf16[512,128]{1,0:T(8,128)(2,1)} %bitcast.16, bf16[512,64]{1,0:T(8,128)(2,1)} %bitcast.11, ...), custom_call_target="tpu_custom_call" | custom-call | tf_op jit(solution)/shard_map/pallas_call | solution.py:535
  141.8 1.9 %copy.21 = bf16[128,2048]{1,0:T(8,128)(2,1)} copy(bf16[128,2048]{1,0:T(8,128)(2,1)} %bitcast.10) | data formatting | bytes 1048576

commit v2 on v1

--- a/solution.py
+++ b/solution.py
@@ -134,6 +134,16 @@
 
 def last(a, b):
     return lax.dot_general(a, b, (((1,), (1,)), ((), ())), preferred_element_type=jnp.float32)
+
+
+def folded(value):
+    middle = value.shape[0] // 2
+    return jnp.concatenate([value[:middle], value[middle:]], axis=1)
+
+
+def unfolded(value):
+    middle = value.shape[1] // 2
+    return jnp.concatenate([value[:, :middle], value[:, middle:]], axis=0)
 
 
 def add(a, b):
@@ -175,6 +185,8 @@
     depth = up_h.shape[0]
     width = up_all.shape[1]
     half = tokens // 2
+    part_depth = depth // 2
+    count_all = line * PLANE
     piece = PLANE * depth
 
     def fetched(number, src, dst):
@@ -183,17 +195,22 @@
     def at_place(ref, number, size):
         return ref.at[pl.ds(pl.multiple_of(number * size, size), size)]
 
-    def columns(ref, number):
-        return ref.at[:, pl.ds(pl.multiple_of(number * width, width), width)]
+    def spot(name, h, number):
+        if name == "up":
+            return up_all.at[pl.ds(pl.multiple_of(number * depth + h * part_depth, part_depth), part_depth)]
+        return down_all.at[pl.ds(pl.multiple_of((h * count_all + number) * part_depth, part_depth), part_depth)]
 
     small = [
         fetched(0, k1_h, k1), fetched(1, v1_h, v1), fetched(2, k2_h, k2), fetched(3, v2_h, v2),
         fetched(4, q1_h, q1), fetched(5, q2_h, q2),
     ]
-    own_up = fetched(6, columns(up_h, z), at_place(up_all, s, depth))
-    own_down = fetched(7, columns(down_h, z), at_place(down_all, s, depth))
-    large = [fetched(8, resid_h, resid), fetched(9, o1_h, o1), fetched(10, o2_h, o2)]
-    for copy in small + [own_up, own_down] + large:
+    own_weights = {}
+    for i, (name, source) in enumerate((("up", up_h), ("down", down_h))):
+        for h in range(2):
+            block = source.at[h * part_depth:(h + 1) * part_depth, pl.ds(pl.multiple_of(z * width, width), width)]
+            own_weights[name, h] = fetched(6 + 2 * i + h, block, spot(name, h, s))
+    large = [fetched(10, resid_h, resid), fetched(11, o1_h, o1), fetched(12, o2_h, o2)]
+    for copy in small + list(own_weights.values()) + large:
         copy.start()
 
     barrier = pltpu.get_barrier_semaphore()
@@ -231,18 +248,29 @@
         moved = jnp.dot(pick, value, preferred_element_type=jnp.float32).astype(jnp.bfloat16)
         return moved.reshape(line, tokens, value.shape[1])
 
+    row = lax.broadcasted_iota(jnp.int32, (tokens, tokens), 0)
+    column = lax.broadcasted_iota(jnp.int32, (tokens, tokens), 1)
+    same = jnp.where(row == column, 1.0, 0.0).astype(jnp.bfloat16)
     kv_own[:, :, 0:wide] = by_head(k1[...])
     kv_own[:, :, wide:2 * wide] = by_head(v1[...])
-    kv_own[:, :, 2 * wide:3 * wide] = by_head(jnp.concatenate([k2[...], v2[...]], axis=1))
-    q_own[:, :, 0:wide] = by_head(q1[...])
-    q_own[:, :, wide:] = by_head(q2[...])
+    for h in range(line):
+        turned = last(same, jnp.concatenate([k2[h], v2[h]], axis=0))
+        kv_own[h, :, 2 * wide:3 * wide] = turned.astype(jnp.bfloat16)
+    q_own[:, 0:tokens, :] = by_head(q1[...])
+    for h in range(line):
+        q_own[h, tokens:, :] = folded(last(same, q2[h]).astype(jnp.bfloat16))
     pl.semaphore_wait(barrier, len(peers))
 
     def ahead(j):
-        return (z + j) % line
-
-    def behind(j):
-        return (z + line - j) % line
+        number = z
+        bit = 1
+        while bit <= j:
+            if j & bit:
+                number = number + bit * (1 - 2 * ((number // bit) % 2))
+            bit *= 2
+        return number
+
+    behind = ahead
 
     def z_peer(j):
         return (ahead(j) * PLANE + p, c)
@@ -252,40 +280,51 @@
         send(kv_own.at[ahead(j)], mine, kzs.at[j], kzr.at[j], z_peer(j))
     send(kv_own.at[z], mine, kps.at[0, 0], kpr.at[0, 0], to_near)
     send(kv_own.at[z], mine, kps.at[0, 1], kpr.at[0, 1], to_side)
-    for j in range(1, line):
-        send(q_own.at[ahead(j)], q_all.at[z], qzs.at[j], qzr.at[j], z_peer(j))
     mine[...] = kv_own[z]
     q_all[z] = q_own[z]
 
-    weights = {
-        "up": (up_h, up_all, own_up, uzs, uzr, ups, upr),
-        "down": (down_h, down_all, own_down, dzs, dzr, dps, dpr),
-    }
-
-    def along(name, j):
-        source, whole, _, ss, sr, _, _ = weights[name]
-        send(columns(source, ahead(j)), at_place(whole, s, depth), ss.at[j], sr.at[j], z_peer(j))
-
-    def spread(name, j):
-        _, whole, own, _, sr, ss, rr_ = weights[name]
-        block = at_place(whole, behind(j) * PLANE + p, depth)
+    def push(name, h, j):
+        source = up_h if name == "up" else down_h
+        block = source.at[h * part_depth:(h + 1) * part_depth, pl.ds(pl.multiple_of(ahead(j) * width, width), width)]
+        ss, sr = (uzs, uzr) if name == "up" else (dzs, dzr)
+        send(block, spot(name, h, s), ss.at[h, j], sr.at[h, j], z_peer(j))
+
+    def plane_sems(name):
+        return (ups, upr) if name == "up" else (dps, dpr)
+
+    def spread(name, h, j):
+        block = spot(name, h, behind(j) * PLANE + p)
         if j:
-            arrived(block, sr.at[j])
+            arrived(block, (uzr if name == "up" else dzr).at[h, j])
         else:
-            own.wait()
-        send(block, block, ss.at[j, 0], rr_.at[j, 0], to_near)
-        send(block, block, ss.at[j, 1], rr_.at[j, 1], to_side)
-
-    def relay(name, j):
-        _, whole, _, _, _, ss, rr_ = weights[name]
-        block = at_place(whole, behind(j) * PLANE + near, depth)
-        arrived(block, rr_.at[j, 0])
-        send(block, block, ss.at[j, 2], rr_.at[j, 2], to_side)
-
-    def settle(name, j):
-        _, whole, _, _, _, _, rr_ = weights[name]
+            own_weights[name, h].wait()
+        ss, sr = plane_sems(name)
+        send(block, block, ss.at[h, j, 0], sr.at[h, j, 0], to_near)
+        send(block, block, ss.at[h, j, 1], sr.at[h, j, 1], to_side)
+
+    def relay(name, h, j):
+        block = spot(name, h, behind(j) * PLANE + near)
+        ss, sr = plane_sems(name)
+        arrived(block, sr.at[h, j, 0])
+        send(block, block, ss.at[h, j, 2], sr.at[h, j, 2], to_side)
+
+    def settle(name, h, j):
+        ss, sr = plane_sems(name)
         for way, where in ((1, side), (2, far)):
-            arrived(at_place(whole, behind(j) * PLANE + where, depth), rr_.at[j, way])
+            arrived(spot(name, h, behind(j) * PLANE + where), sr.at[h, j, way])
+
+    done = []
+
+    def flow(*items):
+        for item in items:
+            spread(*item)
+            if done:
+                relay(*done[-1])
+            done.append(item)
+
+    def ask():
+        for j in range(1, line):
+            send(q_own.at[ahead(j)], q_all.at[z], qzs.at[j], qzr.at[j], z_peer(j))
 
     def kv_spread(j):
         block = at_place(kv_all, behind(j) * PLANE + p, tokens)
@@ -298,21 +337,26 @@
         arrived(block, kpr.at[j, 0])
         send(block, block, kps.at[j, 2], kpr.at[j, 2], to_side)
 
-    for j in range(1, line):
-        along("up", j)
     kv_spread(1)
     kv_relay(0)
+
     kv_spread(2)
+    ask()
+    push("up", 0, 1)
+    push("up", 1, 1)
     kv_relay(1)
     kv_spread(3)
     kv_relay(2)
     kv_relay(3)
-    spread("up", 0)
+
     for j in range(line):
         for way, where in ((1, side), (2, far)):
             arrived(at_place(kv_all, behind(j) * PLANE + where, tokens), kpr.at[j, way])
     for j in range(1, line):
         arrived(q_all.at[behind(j)], qzr.at[j])
+    flow(("up", 0, 0))
+    push("up", 0, 2)
+    push("up", 1, 2)
 
     lanes_a = lax.broadcasted_iota(jnp.int32, (tokens, wide), 1)
     lanes_b = lax.broadcasted_iota(jnp.int32, (tokens, deep), 1)
@@ -343,30 +387,28 @@
     def tile(j):
         number = (j + 1) * span
         first = mix(
-            q_all[j, :, 0:wide], lanes_a, slice(0, wide), slice(wide, 2 * wide), size_a, bal_a[z], number
+            q_all[j, 0:tokens, :], lanes_a, slice(0, wide), slice(wide, 2 * wide), size_a, bal_a[z], number
         )
-        heads_out[j, :, 0:wide] = norm(first, gain_a)
+        heads_out[j, 0:tokens, :] = norm(first, gain_a)
         second = mix(
-            q_all[j, :, wide:], lanes_b, slice(2 * wide, 2 * wide + deep),
+            unfolded(q_all[j, tokens:, :]), lanes_b, slice(2 * wide, 2 * wide + deep),
             slice(2 * wide, 3 * wide), size_b, bal_b[z], number,
         )
-        heads_out[j, :, wide:] = norm(second[:, wide - deep:wide], gain_b)
+        heads_out[j, tokens:, :] = folded(norm(second[:, wide - deep:wide], gain_b))
         send_if(j != z, heads_out.at[j], heads_in.at[z], hzs.at[j], hzr.at[z], (j * PLANE + p, c))
 
     tile(3)
-    relay("up", 0)
+
     tile(2)
-    spread("up", 1)
+    flow(("up", 1, 0))
+    push("up", 0, 3)
     tile(1)
+
     tile(0)
     heads_in[z] = heads_out[z]
-    along("down", 1)
-    along("down", 2)
-    relay("up", 1)
-    spread("up", 2)
-    relay("up", 2)
-    spread("up", 3)
-    spread("down", 0)
+    push("up", 1, 3)
+    push("down", 0, 1)
+    flow(("down", 0, 0), ("down", 1, 0), ("up", 0, 1), ("up", 1, 1))
     for copy in large:
         copy.wait()
     for h in range(line):
@@ -376,8 +418,8 @@
         def _():
             arrived(block, hzr.at[h])
 
-    heads_first = jnp.concatenate([heads_in[h, :, 0:wide] for h in range(line)], axis=1)
-    heads_second = jnp.concatenate([heads_in[h, :, wide:] for h in range(line)], axis=1)
+    heads_first = jnp.concatenate([heads_in[h, 0:tokens, :] for h in range(line)], axis=1)
+    heads_second = jnp.concatenate([unfolded(heads_in[h, tokens:, :]) for h in range(line)], axis=1)
     step = features // 4
     for n in range(4):
         at = slice(n * step, (n + 1) * step)
@@ -387,7 +429,8 @@
         part[:, :, at] = value.astype(jnp.bfloat16).reshape(2, half, step)
     swap = remote(part.at[1 - c], other_part, sws.at[0], swr.at[0], to_core)
     swap.start()
-    relay("up", 3)
+    push("down", 0, 2)
+    flow(("up", 0, 2))
     swap.wait()
     both = part[c].astype(jnp.float32) + other_part[...].astype(jnp.float32)
     mine_rows = pl.ds(pl.multiple_of(c * half, half), half)
@@ -400,10 +443,12 @@
     send_if(z < line - 1, own_slot, own_slot, rus.at[0], rr.at[z], to_up)
     send_if(z > 0, own_slot, own_slot, rds.at[0], rr.at[z], to_down)
     send(own_slot, own_slot, rcs.at[0], rcr.at[z], to_core)
-    relay("down", 0)
-    for d in range(1, line):
-        from_low = at_place(rows, jnp.maximum(z - d, 0) * 2 + c, half)
+
+    def rows_pass(d):
         low = jnp.maximum(z - d, 0)
+        high = jnp.minimum(z + d, line - 1)
+        from_low = at_place(rows, low * 2 + c, half)
+        from_high = at_place(rows, high * 2 + c, half)
 
         @pl.when(z >= d)
         def _():
@@ -411,8 +456,6 @@
 
         send_if((z >= d) & (z < line - 1), from_low, from_low, rus.at[d], rr.at[low], to_up)
         send_if(z >= d, from_low, from_low, rcs.at[d], rcr.at[low], to_core)
-        high = jnp.minimum(z + d, line - 1)
-        from_high = at_place(rows, high * 2 + c, half)
 
         @pl.when(z + d < line)
         def _():
@@ -420,30 +463,32 @@
 
         send_if((z + d < line) & (z > 0), from_high, from_high, rds.at[d], rr.at[high], to_down)
         send_if(z + d < line, from_high, from_high, rcs.at[line - 1 + d], rcr.at[high], to_core)
-        if d == 1:
-            along("down", 3)
-            spread("down", 1)
-        if d == 2:
-            relay("down", 1)
-            spread("down", 2)
-    for k in range(line):
-        arrived(at_place(rows, k * 2 + 1 - c, half), rcr.at[k])
-    for j in range(line):
-        settle("up", j)
-    relay("down", 2)
-
+
+    flow(("up", 1, 2), ("up", 0, 3))
+    rows_pass(1)
+    push("down", 0, 3)
+    push("down", 1, 1)
+    flow(("up", 1, 3), ("down", 0, 1))
+    rows_pass(2)
+    for j in (2, 3):
+        push("down", 1, j)
+    flow(("down", 0, 2), ("down", 0, 3))
+    rows_pass(3)
+    flow(("down", 1, 1))
     lift = 256
 
-    @pl.loop(0, width // lift)
-    def _(n):
-        at = pl.ds(pl.multiple_of(n * lift, lift), lift)
-        lifted = jnp.maximum(jnp.dot(rows[...], up_all[:, at], preferred_element_type=jnp.float32), 0.0)
-        hidden[:, at] = (lifted * lifted).astype(jnp.bfloat16)
-
-    spread("down", 3)
-    relay("down", 3)
-    for j in range(line):
-        settle("down", j)
+    def raise_rows():
+        for k in range(line):
+            arrived(at_place(rows, k * 2 + 1 - c, half), rcr.at[k])
+        for h in range(2):
+            for j in range(line):
+                settle("up", h, j)
+
+        @pl.loop(0, width // lift)
+        def _(n):
+            at = pl.ds(pl.multiple_of(n * lift, lift), lift)
+            lifted = jnp.maximum(jnp.dot(rows[...], up_all[:, at], preferred_element_type=jnp.float32), 0.0)
+            hidden[:, at] = (lifted * lifted).astype(jnp.bfloat16)
 
     def chunk(k):
         at = slice(k * piece, (k + 1) * piece)
@@ -451,34 +496,41 @@
         terms[:, :, :, at] = value.reshape(line, 2, half, piece)
         send(terms.at[:, 1 - c, :, at], held.at[:, :, at], ts.at[k], tr.at[k], to_core)
 
-    def reduce(k):
+    ends = (z == 0) | (z == line - 1)
+    inner = (z > 0) & (z < line - 1)
+
+    def reduce(k, who):
         at = slice(k * piece, (k + 1) * piece)
-        arrived(held.at[:, :, at], tr.at[k])
-        for zd in range(line):
-            acc[zd, :, at] = add(terms[zd, c, :, at], held[zd, :, at])
+
+        @pl.when(who)
+        def _():
+            arrived(held.at[:, :, at], tr.at[k])
+            for zd in range(line):
+                acc[zd, :, at] = add(terms[zd, c, :, at], held[zd, :, at])
+
         for d in range(line - 1, 0, -1):
             high = jnp.minimum(z + d, line - 1)
             block = below.at[high, :, at]
 
-            @pl.when((z + d < line) & (z > 0))
+            @pl.when(who & (z + d < line) & (z > 0))
             def _():
                 arrived(block, cbr.at[high, k])
                 acc[high, :, at] = add(acc[high, :, at], below[high, :, at])
 
-            send_if(z + d < line, acc.at[high, :, at], block, cus.at[d, k], cbr.at[high, k], to_up)
+            send_if(who & (z + d < line), acc.at[high, :, at], block, cus.at[d, k], cbr.at[high, k], to_up)
             low = jnp.maximum(z - d, 0)
             block = above.at[low, :, at]
 
-            @pl.when((z >= d) & (z < line - 1))
+            @pl.when(who & (z >= d) & (z < line - 1))
             def _():
                 arrived(block, car.at[low, k])
                 acc[low, :, at] = add(acc[low, :, at], above[low, :, at])
 
-            send_if(z >= d, acc.at[low, :, at], block, cds.at[d, k], car.at[low, k], to_down)
+            send_if(who & (z >= d), acc.at[low, :, at], block, cds.at[d, k], car.at[low, k], to_down)
 
     def finish(k):
         at = slice(k * piece, (k + 1) * piece)
-        total[...] = mixed[:, at].astype(jnp.float32) + acc[z, :, at].astype(jnp.float32)
+        total[...] = acc[z, :, at].astype(jnp.float32)
 
         @pl.when(z > 0)
         def _():
@@ -490,19 +542,42 @@
             arrived(above.at[z, :, at], car.at[z, k])
             total[...] += above[z, :, at].astype(jnp.float32)
 
-        out[c, :, at] = total[...].astype(jnp.bfloat16)
-        send(out.at[c, :, at], out.at[c, :, at], fs.at[k], fr.at[k], to_core)
-
-    for k in range(line):
-        chunk(k)
-        if k:
-            reduce(k - 1)
-    reduce(line - 1)
-    for k in range(line):
+        h = k // 2
+        value = total[...]
+        for i in range(piece // part_depth):
+            number = (k % 2) * (piece // part_depth) + i
+            to = slice(number * depth + h * part_depth, number * depth + (h + 1) * part_depth)
+            term = value[:, i * part_depth:(i + 1) * part_depth]
+            out[c, :, to] = (mixed[:, to].astype(jnp.float32) + term).astype(jnp.bfloat16)
+        if h:
+            to = slice((k % 2) * 2 * piece, (k % 2 + 1) * 2 * piece)
+            send(out.at[c, :, to], out.at[c, :, to], fs.at[k % 2], fr.at[k % 2], to_core)
+
+    raise_rows()
+    flow(("down", 1, 2))
+    for j in range(line):
+        settle("down", 0, j)
+    chunk(0)
+    chunk(1)
+    flow(("down", 1, 3))
+    reduce(0, ends)
+    reduce(1, ends)
+    relay(*done[-1])
+    for j in range(line):
+        settle("down", 1, j)
+    chunk(2)
+    chunk(3)
+    reduce(0, inner)
+    reduce(1, inner)
+    reduce(2, ends)
+    reduce(3, ends)
+    reduce(2, inner)
+    reduce(3, inner)
+    for k in range(4):
         finish(k)
-    for k in range(line):
-        at = slice(k * piece, (k + 1) * piece)
-        arrived(out.at[1 - c, :, at], fr.at[k])
+    for k in range(2):
+        to = slice(k * 2 * piece, (k + 1) * 2 * piece)
+        arrived(out.at[1 - c, :, to], fr.at[k])
     for condition, copy in sends:
         if condition is None:
             copy.wait_send()
@@ -519,7 +594,6 @@
     tokens, features = residual.shape
     half = tokens // 2
     wide = v1.shape[1]
-    deep = v2.shape[1]
     n = line * PLANE
     width = up.shape[1] // line
     depth = up.shape[0]
@@ -540,23 +614,23 @@
         scratch_shapes=[
             buffer(tokens, features), buffer(*q1.shape), buffer(*k1.shape), buffer(*v1.shape),
             buffer(*q2.shape), buffer(*k2.shape), buffer(*v2.shape), buffer(*o1.shape), buffer(*o2.shape),
-            buffer(line, tokens, 3 * wide), buffer(line, tokens, wide + deep),
-            buffer(n * tokens, 3 * wide), buffer(line, tokens, wide + deep),
-            buffer(line, tokens, wide + deep), buffer(line, tokens, wide + deep),
+            buffer(line, tokens, 3 * wide), buffer(line, tokens + half, wide),
+            buffer(n * tokens, 3 * wide), buffer(line, tokens + half, wide),
+            buffer(line, tokens + half, wide), buffer(line, tokens + half, wide),
             buffer(n * depth, width), buffer(n * depth, width),
             buffer(2, half, features), buffer(half, features), buffer(half, features),
             buffer(line * tokens, features), buffer(line * tokens, width),
             buffer(line, 2, half, features), buffer(line, half, features), buffer(line, half, features),
             buffer(line, half, features), buffer(line, half, features),
             pltpu.VMEM((half, PLANE * depth), jnp.float32),
-            dma((11,)),
+            dma((13,)),
             dma((line,)), dma((line,)), dma((line,)), dma((line,)), dma((line, 3)), dma((line, 3)),
-            dma((line,)), dma((line,)), dma((line, 3)), dma((line, 3)),
-            dma((line,)), dma((line,)), dma((line, 3)), dma((line, 3)),
+            dma((2, line)), dma((2, line)), dma((2, line, 3)), dma((2, line, 3)),
+            dma((2, line)), dma((2, line)), dma((2, line, 3)), dma((2, line, 3)),
             dma((line,)), dma((line,)), dma((1,)), dma((1,)),
             dma((line,)), dma((line,)), dma((line,)), dma((2 * line - 1,)), dma((line,)),
             dma((line,)), dma((line,)), dma((line, line)), dma((line, line)),
-            dma((line, line)), dma((line, line)), dma((line,)), dma((line,)),
+            dma((line, line)), dma((line, line)), dma((2,)), dma((2,)),
         ],
         compiler_params=pltpu.CompilerParams(
             collective_id=0, has_side_effects=True, vmem_limit_bytes=60 * 1024 * 1024
@@ -574,9 +648,12 @@
     def flat(array):
         return array.reshape(tokens * line, array.shape[2])
 
+    def turned(array):
+        return array.transpose(1, 2, 0)
+
     out = layer(
-        line, residual, flat(query_first), flat(key_first), flat(value_first), flat(query_second),
-        flat(key_second), flat(value_second), balance_first, balance_second,
+        line, residual, flat(query_first), flat(key_first), flat(value_first), turned(query_second),
+        turned(key_second), turned(value_second), balance_first, balance_second,
         head_gain_first[None, :], head_gain_second[None, :], out_first, out_second,
         mlp_gain[None, :], up_weight, down_weight,
     )
@@ -596,10 +673,11 @@
         query_first, query_second, value_second, value_first = arrays[1], arrays[4], arrays[6], arrays[3]
         fits = (
             placed(mesh)
+            and ranks & (ranks - 1) == 0
             and query_first.shape[1] * PLANE == ranks
             and query_second.shape[1] == query_first.shape[1]
             and value_first.shape[2] == query_first.shape[2] == 128
-            and query_second.shape[2] + value_second.shape[2] == query_first.shape[2]
+            and query_second.shape[2] * 2 == value_second.shape[2] * 2 == query_first.shape[2]
             and query_first.shape[0] % 32 == 0
             and arrays[14].shape[1] % (128 * ranks) == 0
         )

time: 144 us -> 128 us (0.89)
  Pallas kernels: 137 us -> 126 us
  local copies, waits for them, and re-layouts: 6.71 us -> 1.88 us
    pallas_call x1, Pallas kernels: 137 us -> 126 us  [layer(): pl.pallas_call(functools.partial(layer_kernel, line, q1.shape[1] // 2, q2...]
    unnamed x4 -> x1, local copies, waits for them, and re-layouts: 6.71 us -> 1.88 us
where the time goes in v2:
time: 128 us
  Pallas kernels  126 us (98%)
  local copies, waits for them, and re-layouts  1.88 us (1%)
    pallas_call x1, Pallas kernels, layer(): pl.pallas_call(functools.partial(layer_kernel, line, q1.shape[1] // 2, q2...  126 us

profile of v2, /device:TPU:0, one launch (start us, length us, event | category | flops | bytes accessed | tf_op | source)
XLA Modules:
  0.0 128.0 jit_solution(6710303944429012520)
XLA Ops:
  0.0 126.1 %shard_map.154 = bf16[2,64,2048]{2,1,0:T(8,128)(2,1)} custom-call(f32[4]{0:T(128)} %bal_a.1, f32[4]{0:T(128)} %bal_b.1, bf16[128,2048]{1,0:T(8,128)(2,1)} %resid_h.1, bf16[512,128]{1,0:T(8,128)(2,1)} %bitcast.11, bf16[512,128]{1,0:T(8,128)(2,1)} %bitcast.12, bf16[512,128]{1,0:T(8,128)(2,1)} %bitcast.13, bf16[4,64,128]{2,1,0:T(8,128)(2,1)} %bitcast.14, ...), custom_call_target="tpu_custom_call" | custom-call | tf_op jit(solution)/shard_map/pallas_call | solution.py:609
  126.2 1.9 %copy.18 = bf16[128,2048]{1,0:T(8,128)(2,1)} copy(bf16[128,2048]{1,0:T(8,128)(2,1)} %bitcast.10) | data formatting | bytes 1048576

commit v3 on v2

--- a/solution.py
+++ b/solution.py
@@ -156,7 +156,7 @@
     mlp_gain, up_h, down_h,
     out,
     resid, q1, k1, v1, q2, k2, v2, o1, o2, kv_own, q_own, kv_all, q_all, heads_out, heads_in,
-    up_all, down_all, part, other_part, mixed, rows, hidden, terms, held, acc, below, above, total,
+    up_all, down_all, part, other_part, mixed, rows, hidden, terms, held, acc, relays, from_mate, from_across, result,
     fetch, kzs, kzr, qzs, qzr, kps, kpr, uzs, uzr, ups, upr, dzs, dzr, dps, dpr, hzs, hzr,
     sws, swr, rus, rds, rr, rcs, rcr, ts, tr, cus, cds, cbr, car, fs, fr,
 ):
@@ -185,7 +185,8 @@
     depth = up_h.shape[0]
     width = up_all.shape[1]
     half = tokens // 2
-    part_depth = depth // 2
+    stages = {"up": 2, "down": line}
+    share = {name: depth // number for name, number in stages.items()}
     count_all = line * PLANE
     piece = PLANE * depth
 
@@ -196,9 +197,10 @@
         return ref.at[pl.ds(pl.multiple_of(number * size, size), size)]
 
     def spot(name, h, number):
+        size = share[name]
         if name == "up":
-            return up_all.at[pl.ds(pl.multiple_of(number * depth + h * part_depth, part_depth), part_depth)]
-        return down_all.at[pl.ds(pl.multiple_of((h * count_all + number) * part_depth, part_depth), part_depth)]
+            return up_all.at[pl.ds(pl.multiple_of(number * depth + h * size, size), size)]
+        return down_all.at[pl.ds(pl.multiple_of((h * count_all + number) * size, size), size)]
 
     small = [
         fetched(0, k1_h, k1), fetched(1, v1_h, v1), fetched(2, k2_h, k2), fetched(3, v2_h, v2),
@@ -206,10 +208,11 @@
     ]
     own_weights = {}
     for i, (name, source) in enumerate((("up", up_h), ("down", down_h))):
-        for h in range(2):
-            block = source.at[h * part_depth:(h + 1) * part_depth, pl.ds(pl.multiple_of(z * width, width), width)]
-            own_weights[name, h] = fetched(6 + 2 * i + h, block, spot(name, h, s))
-    large = [fetched(10, resid_h, resid), fetched(11, o1_h, o1), fetched(12, o2_h, o2)]
+        for h in range(stages[name]):
+            rows_at = slice(h * share[name], (h + 1) * share[name])
+            block = source.at[rows_at, pl.ds(pl.multiple_of(z * width, width), width)]
+            own_weights[name, h] = fetched(9 + 2 * i + h, block, spot(name, h, s))
+    large = [fetched(6, resid_h, resid), fetched(7, o1_h, o1), fetched(8, o2_h, o2)]
     for copy in small + list(own_weights.values()) + large:
         copy.start()
 
@@ -285,7 +288,8 @@
 
     def push(name, h, j):
         source = up_h if name == "up" else down_h
-        block = source.at[h * part_depth:(h + 1) * part_depth, pl.ds(pl.multiple_of(ahead(j) * width, width), width)]
+        rows_at = slice(h * share[name], (h + 1) * share[name])
+        block = source.at[rows_at, pl.ds(pl.multiple_of(ahead(j) * width, width), width)]
         ss, sr = (uzs, uzr) if name == "up" else (dzs, dzr)
         send(block, spot(name, h, s), ss.at[h, j], sr.at[h, j], z_peer(j))
 
@@ -314,13 +318,18 @@
             arrived(spot(name, h, behind(j) * PLANE + where), sr.at[h, j, way])
 
     done = []
+    lag = 2
 
     def flow(*items):
         for item in items:
             spread(*item)
-            if done:
-                relay(*done[-1])
+            if len(done) >= lag:
+                relay(*done[-lag])
             done.append(item)
+
+    def drain():
+        for item in done[-lag:]:
+            relay(*item)
 
     def ask():
         for j in range(1, line):
@@ -339,16 +348,16 @@
 
     kv_spread(1)
     kv_relay(0)
-
     kv_spread(2)
+    kv_relay(1)
+    kv_spread(3)
+    push("down", 2, 3)
     ask()
     push("up", 0, 1)
     push("up", 1, 1)
-    kv_relay(1)
-    kv_spread(3)
+    push("down", 3, 3)
     kv_relay(2)
     kv_relay(3)
-
     for j in range(line):
         for way, where in ((1, side), (2, far)):
             arrived(at_place(kv_all, behind(j) * PLANE + where, tokens), kpr.at[j, way])
@@ -356,29 +365,30 @@
         arrived(q_all.at[behind(j)], qzr.at[j])
     flow(("up", 0, 0))
     push("up", 0, 2)
-    push("up", 1, 2)
 
     lanes_a = lax.broadcasted_iota(jnp.int32, (tokens, wide), 1)
     lanes_b = lax.broadcasted_iota(jnp.int32, (tokens, deep), 1)
-    line_rows = lax.broadcasted_iota(jnp.int32, (tokens, span), 0) + p * tokens
-    visible = lax.broadcasted_iota(jnp.int32, (tokens, span), 1) <= line_rows
+    line_rows = lax.broadcasted_iota(jnp.int32, (2 * tokens, span), 0) % tokens + p * tokens
+    visible = lax.broadcasted_iota(jnp.int32, (2 * tokens, span), 1) <= line_rows
 
     def mix(queries, lanes, keys_at, values_at, size, b, keys_number):
-        maps = []
-        for m in range(2):
-            chosen = (lanes >= m * size) & (lanes < (m + 1) * size)
-            picked = jnp.where(chosen, queries, jnp.zeros_like(queries))
-            scores = last(picked, kv_all[0:keys_number, keys_at]) * size ** (-0.5)
-            tail_scores = jnp.where(visible, scores[:, keys_number - span:], -jnp.inf)
-            if keys_number > span:
-                scores = jnp.concatenate([scores[:, : keys_number - span], tail_scores], axis=1)
-            else:
-                scores = tail_scores
-            powers = jnp.exp(scores - jnp.max(scores, axis=-1, keepdims=True))
-            maps.append((powers, jnp.sum(powers, axis=-1, keepdims=True)))
-        (e1, l1), (e2, l2) = maps
-        mixing = (e1 * (1.0 / l1) - e2 * (b / l2)).astype(jnp.bfloat16)
-        return jnp.dot(mixing, kv_all[0:keys_number, values_at], preferred_element_type=jnp.float32)
+        zeros = jnp.zeros_like(queries)
+        picked = jnp.concatenate(
+            [jnp.where(lanes < size, queries, zeros), jnp.where(lanes < size, zeros, queries)], axis=0
+        )
+        scores = last(picked, kv_all[0:keys_number, keys_at])
+        tail_scores = jnp.where(visible, scores[:, keys_number - span:], -jnp.inf)
+        if keys_number > span:
+            scores = jnp.concatenate([scores[:, : keys_number - span], tail_scores], axis=1)
+        else:
+            scores = tail_scores
+        gaps = scores - jnp.max(scores, axis=-1, keepdims=True)
+        powers = jnp.exp2(gaps * (size ** (-0.5) * math.log2(math.e)))
+        sums = jnp.sum(powers, axis=-1, keepdims=True)
+        both = jnp.dot(
+            powers.astype(jnp.bfloat16), kv_all[0:keys_number, values_at], preferred_element_type=jnp.float32
+        )
+        return both[:tokens] * (1.0 / sums[:tokens]) - both[tokens:] * (b / sums[tokens:])
 
     def norm(value, gain):
         power = jnp.mean(value * value, axis=-1, keepdims=True)
@@ -401,14 +411,21 @@
 
     tile(2)
     flow(("up", 1, 0))
-    push("up", 0, 3)
+    push("up", 1, 2)
     tile(1)
 
     tile(0)
     heads_in[z] = heads_out[z]
+    push("up", 0, 3)
+    push("down", 0, 1)
+    push("down", 1, 1)
+    flow(("down", 0, 0))
+    flow(("down", 1, 0))
+    flow(("down", 2, 0))
+    flow(("down", 3, 0))
     push("up", 1, 3)
-    push("down", 0, 1)
-    flow(("down", 0, 0), ("down", 1, 0), ("up", 0, 1), ("up", 1, 1))
+    flow(("up", 0, 1))
+    flow(("up", 1, 1))
     for copy in large:
         copy.wait()
     for h in range(line):
@@ -429,7 +446,6 @@
         part[:, :, at] = value.astype(jnp.bfloat16).reshape(2, half, step)
     swap = remote(part.at[1 - c], other_part, sws.at[0], swr.at[0], to_core)
     swap.start()
-    push("down", 0, 2)
     flow(("up", 0, 2))
     swap.wait()
     both = part[c].astype(jnp.float32) + other_part[...].astype(jnp.float32)
@@ -444,11 +460,9 @@
     send_if(z > 0, own_slot, own_slot, rds.at[0], rr.at[z], to_down)
     send(own_slot, own_slot, rcs.at[0], rcr.at[z], to_core)
 
-    def rows_pass(d):
+    def rows_low(d):
         low = jnp.maximum(z - d, 0)
-        high = jnp.minimum(z + d, line - 1)
         from_low = at_place(rows, low * 2 + c, half)
-        from_high = at_place(rows, high * 2 + c, half)
 
         @pl.when(z >= d)
         def _():
@@ -457,6 +471,10 @@
         send_if((z >= d) & (z < line - 1), from_low, from_low, rus.at[d], rr.at[low], to_up)
         send_if(z >= d, from_low, from_low, rcs.at[d], rcr.at[low], to_core)
 
+    def rows_high(d):
+        high = jnp.minimum(z + d, line - 1)
+        from_high = at_place(rows, high * 2 + c, half)
+
         @pl.when(z + d < line)
         def _():
             arrived(from_high, rr.at[high])
@@ -464,17 +482,31 @@
         send_if((z + d < line) & (z > 0), from_high, from_high, rds.at[d], rr.at[high], to_down)
         send_if(z + d < line, from_high, from_high, rcs.at[line - 1 + d], rcr.at[high], to_core)
 
-    flow(("up", 1, 2), ("up", 0, 3))
-    rows_pass(1)
+    flow(("up", 1, 2))
+    flow(("up", 0, 3))
+    push("down", 0, 2)
+    push("down", 1, 2)
+    rows_low(1)
+    rows_high(1)
     push("down", 0, 3)
-    push("down", 1, 1)
-    flow(("up", 1, 3), ("down", 0, 1))
-    rows_pass(2)
-    for j in (2, 3):
-        push("down", 1, j)
-    flow(("down", 0, 2), ("down", 0, 3))
-    rows_pass(3)
+    push("down", 1, 3)
+    push("down", 2, 1)
+    flow(("up", 1, 3))
+    flow(("down", 0, 1))
     flow(("down", 1, 1))
+    push("down", 3, 1)
+    rows_low(2)
+    rows_high(2)
+    flow(("down", 1, 2))
+    push("down", 2, 2)
+    push("down", 3, 2)
+    flow(("down", 0, 2))
+    flow(("down", 0, 3))
+    flow(("down", 1, 3))
+    rows_low(3)
+    rows_high(3)
+    flow(("down", 2, 1))
+    flow(("down", 3, 1))
     lift = 256
 
     def raise_rows():
@@ -496,88 +528,85 @@
         terms[:, :, :, at] = value.reshape(line, 2, half, piece)
         send(terms.at[:, 1 - c, :, at], held.at[:, :, at], ts.at[k], tr.at[k], to_core)
 
+    upper = z // 2
     ends = (z == 0) | (z == line - 1)
     inner = (z > 0) & (z < line - 1)
-
-    def reduce(k, who):
+    mate = ahead(1)
+    to_mate = (mate * PLANE + p, c)
+    across = [2 - upper, (1 - upper) * (line - 1)]
+
+    def combine(k):
         at = slice(k * piece, (k + 1) * piece)
-
-        @pl.when(who)
-        def _():
-            arrived(held.at[:, :, at], tr.at[k])
-            for zd in range(line):
-                acc[zd, :, at] = add(terms[zd, c, :, at], held[zd, :, at])
-
-        for d in range(line - 1, 0, -1):
-            high = jnp.minimum(z + d, line - 1)
-            block = below.at[high, :, at]
-
-            @pl.when(who & (z + d < line) & (z > 0))
+        arrived(held.at[:, :, at], tr.at[k])
+        for zd in range(line):
+            acc[zd, :, at] = add(terms[zd, c, :, at], held[zd, :, at])
+        for r in (1, 0):
+            block = acc.at[across[r], :, at]
+            send_if(ends, block, relays.at[r, :, at], cus.at[r, k], cbr.at[r, k], to_mate)
+        send(acc.at[mate, :, at], from_mate.at[:, at], cds.at[0, k], car.at[0, k], to_mate)
+
+    def cross(k):
+        at = slice(k * piece, (k + 1) * piece)
+        for r in (1, 0):
+            block = acc.at[across[r], :, at]
+
+            @pl.when(inner)
             def _():
-                arrived(block, cbr.at[high, k])
-                acc[high, :, at] = add(acc[high, :, at], below[high, :, at])
-
-            send_if(who & (z + d < line), acc.at[high, :, at], block, cus.at[d, k], cbr.at[high, k], to_up)
-            low = jnp.maximum(z - d, 0)
-            block = above.at[low, :, at]
-
-            @pl.when(who & (z >= d) & (z < line - 1))
-            def _():
-                arrived(block, car.at[low, k])
-                acc[low, :, at] = add(acc[low, :, at], above[low, :, at])
-
-            send_if(who & (z >= d), acc.at[low, :, at], block, cds.at[d, k], car.at[low, k], to_down)
+                arrived(relays.at[r, :, at], cbr.at[r, k])
+                block[...] = add(block[...], relays[r, :, at])
+
+            send_if(
+                inner, block, from_across.at[:, at], cus.at[2 + r, k], car.at[1, k],
+                (across[r] * PLANE + p, c),
+            )
 
     def finish(k):
         at = slice(k * piece, (k + 1) * piece)
-        total[...] = acc[z, :, at].astype(jnp.float32)
-
-        @pl.when(z > 0)
-        def _():
-            arrived(below.at[z, :, at], cbr.at[z, k])
-            total[...] += below[z, :, at].astype(jnp.float32)
-
-        @pl.when(z < line - 1)
-        def _():
-            arrived(above.at[z, :, at], car.at[z, k])
-            total[...] += above[z, :, at].astype(jnp.float32)
-
-        h = k // 2
-        value = total[...]
-        for i in range(piece // part_depth):
-            number = (k % 2) * (piece // part_depth) + i
-            to = slice(number * depth + h * part_depth, number * depth + (h + 1) * part_depth)
-            term = value[:, i * part_depth:(i + 1) * part_depth]
-            out[c, :, to] = (mixed[:, to].astype(jnp.float32) + term).astype(jnp.bfloat16)
-        if h:
-            to = slice((k % 2) * 2 * piece, (k % 2 + 1) * 2 * piece)
-            send(out.at[c, :, to], out.at[c, :, to], fs.at[k % 2], fr.at[k % 2], to_core)
+        arrived(from_mate.at[:, at], car.at[0, k])
+        arrived(from_across.at[:, at], car.at[1, k])
+        value = acc[z, :, at].astype(jnp.float32) + from_mate[:, at].astype(jnp.float32)
+        value = value + from_across[:, at].astype(jnp.float32)
+        size = share["down"]
+        for i in range(count_all):
+            to = slice(i * depth + k * size, i * depth + (k + 1) * size)
+            term = value[:, i * size:(i + 1) * size]
+            result[:, to] = (mixed[:, to].astype(jnp.float32) + term).astype(jnp.bfloat16)
+        if k == line - 1:
+            send(result, out.at[c], fs.at[0], fr.at[0], to_core)
+            fetched(10 + line, result, out.at[c]).start()
 
     raise_rows()
-    flow(("down", 1, 2))
+    flow(("down", 2, 2))
     for j in range(line):
         settle("down", 0, j)
     chunk(0)
-    chunk(1)
-    flow(("down", 1, 3))
-    reduce(0, ends)
-    reduce(1, ends)
-    relay(*done[-1])
     for j in range(line):
         settle("down", 1, j)
+    chunk(1)
+    flow(("down", 2, 3))
+    combine(0)
+    combine(1)
+    flow(("down", 3, 2))
+    flow(("down", 3, 3))
+    drain()
+    cross(0)
+    for j in range(line):
+        settle("down", 2, j)
     chunk(2)
+    combine(2)
+    cross(1)
+    for j in range(line):
+        settle("down", 3, j)
     chunk(3)
-    reduce(0, inner)
-    reduce(1, inner)
-    reduce(2, ends)
-    reduce(3, ends)
-    reduce(2, inner)
-    reduce(3, inner)
-    for k in range(4):
-        finish(k)
-    for k in range(2):
-        to = slice(k * 2 * piece, (k + 1) * 2 * piece)
-        arrived(out.at[1 - c, :, to], fr.at[k])
+    combine(3)
+    finish(0)
+    finish(1)
+    cross(2)
+    cross(3)
+    finish(2)
+    finish(3)
+    arrived(out.at[1 - c], fr.at[0])
+    fetched(10 + line, result, out.at[c]).wait()
     for condition, copy in sends:
         if condition is None:
             copy.wait_send()
@@ -610,7 +639,7 @@
         functools.partial(layer_kernel, line, q1.shape[1] // 2, q2.shape[1] // 2),
         out_shape=jax.ShapeDtypeStruct((2, half, features), b16),
         in_specs=[smem, smem] + [any_] * 7 + [vmem, vmem, any_, any_, vmem, any_, any_],
-        out_specs=vmem,
+        out_specs=any_,
         scratch_shapes=[
             buffer(tokens, features), buffer(*q1.shape), buffer(*k1.shape), buffer(*v1.shape),
             buffer(*q2.shape), buffer(*k2.shape), buffer(*v2.shape), buffer(*o1.shape), buffer(*o2.shape),
@@ -621,16 +650,15 @@
             buffer(2, half, features), buffer(half, features), buffer(half, features),
             buffer(line * tokens, features), buffer(line * tokens, width),
             buffer(line, 2, half, features), buffer(line, half, features), buffer(line, half, features),
-            buffer(line, half, features), buffer(line, half, features),
-            pltpu.VMEM((half, PLANE * depth), jnp.float32),
-            dma((13,)),
+            buffer(2, half, features), buffer(half, features), buffer(half, features), buffer(half, features),
+            dma((11 + line,)),
             dma((line,)), dma((line,)), dma((line,)), dma((line,)), dma((line, 3)), dma((line, 3)),
             dma((2, line)), dma((2, line)), dma((2, line, 3)), dma((2, line, 3)),
-            dma((2, line)), dma((2, line)), dma((2, line, 3)), dma((2, line, 3)),
+            dma((line, line)), dma((line, line)), dma((line, line, 3)), dma((line, line, 3)),
             dma((line,)), dma((line,)), dma((1,)), dma((1,)),
             dma((line,)), dma((line,)), dma((line,)), dma((2 * line - 1,)), dma((line,)),
-            dma((line,)), dma((line,)), dma((line, line)), dma((line, line)),
-            dma((line, line)), dma((line, line)), dma((2,)), dma((2,)),
+            dma((line,)), dma((line,)), dma((line, line)), dma((1, line)),
+            dma((2, line)), dma((2, line)), dma((1,)), dma((1,)),
         ],
         compiler_params=pltpu.CompilerParams(
             collective_id=0, has_side_effects=True, vmem_limit_bytes=60 * 1024 * 1024

time: 128 us -> 119 us (0.930)
  Pallas kernels: 126 us -> 116 us
    pallas_call x1, Pallas kernels: 126 us -> 116 us  [layer(): pl.pallas_call(functools.partial(layer_kernel, line, q1.shape[1] // 2, q2...]
where the time goes in v3:
time: 119 us; the launch traced here: 118 us
  Pallas kernels  116 us (97%)
  local copies, waits for them, and re-layouts  1.88 us (2%)
    pallas_call x1, Pallas kernels, layer(): pl.pallas_call(functools.partial(layer_kernel, line, q1.shape[1] // 2, q2...  116 us

profile of v3, /device:TPU:0, one launch (start us, length us, event | category | flops | bytes accessed | tf_op | source)
XLA Modules:
  0.0 118.4 jit_solution(13182360250543859726)
XLA Ops:
  0.0 116.5 %shard_map.154 = bf16[2,64,2048]{2,1,0:T(8,128)(2,1)} custom-call(f32[4]{0:T(128)} %bal_a.1, f32[4]{0:T(128)} %bal_b.1, bf16[128,2048]{1,0:T(8,128)(2,1)} %resid_h.1, bf16[512,128]{1,0:T(8,128)(2,1)} %bitcast.11, bf16[512,128]{1,0:T(8,128)(2,1)} %bitcast.12, bf16[512,128]{1,0:T(8,128)(2,1)} %bitcast.13, bf16[4,64,128]{2,1,0:T(8,128)(2,1)} %bitcast.14, ...), custom_call_target="tpu_custom_call" | custom-call | tf_op jit(solution)/shard_map/pallas_call | solution.py:638
  116.5 1.9 %copy.18 = bf16[128,2048]{1,0:T(8,128)(2,1)} copy(bf16[128,2048]{1,0:T(8,128)(2,1)} %bitcast.10) | data formatting | bytes 1048576

commit v4 on v3

--- a/solution.py
+++ b/solution.py
@@ -185,10 +185,18 @@
     depth = up_h.shape[0]
     width = up_all.shape[1]
     half = tokens // 2
-    stages = {"up": 2, "down": line}
-    share = {name: depth // number for name, number in stages.items()}
+    unit = depth // 8
+    sizes = {"up": (4 * unit, 4 * unit), "down": tuple(n * unit for n in (2, 2, 2, 2))}
     count_all = line * PLANE
-    piece = PLANE * depth
+
+    def begin(name, h):
+        return sum(sizes[name][:h])
+
+    def rows_of(name, h):
+        return slice(begin(name, h), begin(name, h) + sizes[name][h])
+
+    def columns_of(k):
+        return slice(count_all * begin("down", k), count_all * begin("down", k + 1))
 
     def fetched(number, src, dst):
         return pltpu.make_async_copy(src, dst, fetch.at[number])
@@ -197,10 +205,10 @@
         return ref.at[pl.ds(pl.multiple_of(number * size, size), size)]
 
     def spot(name, h, number):
-        size = share[name]
+        size = sizes[name][h]
         if name == "up":
-            return up_all.at[pl.ds(pl.multiple_of(number * depth + h * size, size), size)]
-        return down_all.at[pl.ds(pl.multiple_of((h * count_all + number) * size, size), size)]
+            return up_all.at[pl.ds(pl.multiple_of(number * depth + begin(name, h), unit), size)]
+        return down_all.at[pl.ds(pl.multiple_of(count_all * begin(name, h) + number * size, unit), size)]
 
     small = [
         fetched(0, k1_h, k1), fetched(1, v1_h, v1), fetched(2, k2_h, k2), fetched(3, v2_h, v2),
@@ -208,9 +216,8 @@
     ]
     own_weights = {}
     for i, (name, source) in enumerate((("up", up_h), ("down", down_h))):
-        for h in range(stages[name]):
-            rows_at = slice(h * share[name], (h + 1) * share[name])
-            block = source.at[rows_at, pl.ds(pl.multiple_of(z * width, width), width)]
+        for h in range(len(sizes[name])):
+            block = source.at[rows_of(name, h), pl.ds(pl.multiple_of(z * width, width), width)]
             own_weights[name, h] = fetched(9 + 2 * i + h, block, spot(name, h, s))
     large = [fetched(6, resid_h, resid), fetched(7, o1_h, o1), fetched(8, o2_h, o2)]
     for copy in small + list(own_weights.values()) + large:
@@ -288,8 +295,7 @@
 
     def push(name, h, j):
         source = up_h if name == "up" else down_h
-        rows_at = slice(h * share[name], (h + 1) * share[name])
-        block = source.at[rows_at, pl.ds(pl.multiple_of(ahead(j) * width, width), width)]
+        block = source.at[rows_of(name, h), pl.ds(pl.multiple_of(ahead(j) * width, width), width)]
         ss, sr = (uzs, uzr) if name == "up" else (dzs, dzr)
         send(block, spot(name, h, s), ss.at[h, j], sr.at[h, j], z_peer(j))
 
@@ -348,16 +354,16 @@
 
     kv_spread(1)
     kv_relay(0)
+    ask()
     kv_spread(2)
     kv_relay(1)
+    push("up", 0, 1)
     kv_spread(3)
     push("down", 2, 3)
-    ask()
-    push("up", 0, 1)
     push("up", 1, 1)
-    push("down", 3, 3)
     kv_relay(2)
     kv_relay(3)
+    push("down", 3, 3)
     for j in range(line):
         for way, where in ((1, side), (2, far)):
             arrived(at_place(kv_all, behind(j) * PLANE + where, tokens), kpr.at[j, way])
@@ -385,10 +391,10 @@
         gaps = scores - jnp.max(scores, axis=-1, keepdims=True)
         powers = jnp.exp2(gaps * (size ** (-0.5) * math.log2(math.e)))
         sums = jnp.sum(powers, axis=-1, keepdims=True)
-        both = jnp.dot(
-            powers.astype(jnp.bfloat16), kv_all[0:keys_number, values_at], preferred_element_type=jnp.float32
-        )
-        return both[:tokens] * (1.0 / sums[:tokens]) - both[tokens:] * (b / sums[tokens:])
+        mixing = powers[:tokens] * (1.0 / sums[:tokens]) - powers[tokens:] * (b / sums[tokens:])
+        return jnp.dot(
+            mixing.astype(jnp.bfloat16), kv_all[0:keys_number, values_at], preferred_element_type=jnp.float32
+        )
 
     def norm(value, gain):
         power = jnp.mean(value * value, axis=-1, keepdims=True)
@@ -422,9 +428,9 @@
     flow(("down", 0, 0))
     flow(("down", 1, 0))
     flow(("down", 2, 0))
-    flow(("down", 3, 0))
     push("up", 1, 3)
     flow(("up", 0, 1))
+    flow(("down", 3, 0))
     flow(("up", 1, 1))
     for copy in large:
         copy.wait()
@@ -523,9 +529,9 @@
             hidden[:, at] = (lifted * lifted).astype(jnp.bfloat16)
 
     def chunk(k):
-        at = slice(k * piece, (k + 1) * piece)
-        value = last(hidden[...], down_all[k * piece:(k + 1) * piece, :]).astype(jnp.bfloat16)
-        terms[:, :, :, at] = value.reshape(line, 2, half, piece)
+        at = columns_of(k)
+        value = last(hidden[...], down_all[at, :]).astype(jnp.bfloat16)
+        terms[:, :, :, at] = value.reshape(line, 2, half, at.stop - at.start)
         send(terms.at[:, 1 - c, :, at], held.at[:, :, at], ts.at[k], tr.at[k], to_core)
 
     upper = z // 2
@@ -536,7 +542,7 @@
     across = [2 - upper, (1 - upper) * (line - 1)]
 
     def combine(k):
-        at = slice(k * piece, (k + 1) * piece)
+        at = columns_of(k)
         arrived(held.at[:, :, at], tr.at[k])
         for zd in range(line):
             acc[zd, :, at] = add(terms[zd, c, :, at], held[zd, :, at])
@@ -546,7 +552,7 @@
         send(acc.at[mate, :, at], from_mate.at[:, at], cds.at[0, k], car.at[0, k], to_mate)
 
     def cross(k):
-        at = slice(k * piece, (k + 1) * piece)
+        at = columns_of(k)
         for r in (1, 0):
             block = acc.at[across[r], :, at]
 
@@ -561,14 +567,14 @@
             )
 
     def finish(k):
-        at = slice(k * piece, (k + 1) * piece)
+        at = columns_of(k)
         arrived(from_mate.at[:, at], car.at[0, k])
         arrived(from_across.at[:, at], car.at[1, k])
         value = acc[z, :, at].astype(jnp.float32) + from_mate[:, at].astype(jnp.float32)
         value = value + from_across[:, at].astype(jnp.float32)
-        size = share["down"]
+        size = sizes["down"][k]
         for i in range(count_all):
-            to = slice(i * depth + k * size, i * depth + (k + 1) * size)
+            to = slice(i * depth + begin("down", k), i * depth + begin("down", k + 1))
             term = value[:, i * size:(i + 1) * size]
             result[:, to] = (mixed[:, to].astype(jnp.float32) + term).astype(jnp.bfloat16)
         if k == line - 1:
@@ -600,8 +606,8 @@
     chunk(3)
     combine(3)
     finish(0)
+    cross(2)
     finish(1)
-    cross(2)
     cross(3)
     finish(2)
     finish(3)
@@ -701,7 +707,8 @@
         query_first, query_second, value_second, value_first = arrays[1], arrays[4], arrays[6], arrays[3]
         fits = (
             placed(mesh)
-            and ranks & (ranks - 1) == 0
+            and ranks == PLANE * PLANE
+            and arrays[14].shape[0] % 128 == 0
             and query_first.shape[1] * PLANE == ranks
             and query_second.shape[1] == query_first.shape[1]
             and value_first.shape[2] == query_first.shape[2] == 128

time: 119 us -> 118 us (level)
  no operation moved by 1% of the time
where the time goes in v4:
time: 118 us
  Pallas kernels  116 us (98%)
  local copies, waits for them, and re-layouts  1.88 us (2%)
    pallas_call x1, Pallas kernels, layer(): pl.pallas_call(functools.partial(layer_kernel, line, q1.shape[1] // 2, q2...  116 us

profile of v4, /device:TPU:0, one launch (start us, length us, event | category | flops | bytes accessed | tf_op | source)
XLA Modules:
  0.0 117.5 jit_solution(11631768181901658395)
XLA Ops:
  0.0 115.6 %shard_map.154 = bf16[2,64,2048]{2,1,0:T(8,128)(2,1)} custom-call(f32[4]{0:T(128)} %bal_a.1, f32[4]{0:T(128)} %bal_b.1, bf16[128,2048]{1,0:T(8,128)(2,1)} %resid_h.1, bf16[512,128]{1,0:T(8,128)(2,1)} %bitcast.11, bf16[512,128]{1,0:T(8,128)(2,1)} %bitcast.12, bf16[512,128]{1,0:T(8,128)(2,1)} %bitcast.13, bf16[4,64,128]{2,1,0:T(8,128)(2,1)} %bitcast.14, ...), custom_call_target="tpu_custom_call" | custom-call | tf_op jit(solution)/shard_map/pallas_call | solution.py:644
  115.6 1.9 %copy.18 = bf16[128,2048]{1,0:T(8,128)(2,1)} copy(bf16[128,2048]{1,0:T(8,128)(2,1)} %bitcast.10) | data formatting | bytes 1048576
